TPU v7x, 32 devices: a whole 2x2x4 slice. The times are simulated.
32 devices in a mesh: sp: 16 (over z, y, x), tp: 2 (over core).
Axes of the slice: x: 2, y: 2, z: 4, core: 2. Of those that a mesh axis runs over, the one named last changes fastest.
Arguments:
- tokens: bfloat16 [6144, 4096], P(('sp', 'tp')), may hold values from -6 to 6
- norm_gain: float32 [4096], replicated, may hold values from 0.1 to 1.9
- conv_val_w: bfloat16 [4096, 1024], P('sp', 'tp'), may hold values from -0.09375 to 0.09375
- conv_gate_w: bfloat16 [4096, 1024], P('sp', 'tp'), may hold values from -0.09375 to 0.09375
- rec_gate_w: bfloat16 [4096, 1536], P('sp', 'tp'), may hold values from -0.09375 to 0.09375
- rec_in_w: bfloat16 [4096, 1536], P('sp', 'tp'), may hold values from -0.09375 to 0.09375
- conv_taps: bfloat16 [31, 1024], P(None, 'tp'), may hold values from -3 to 3
- conv_bias: float32 [1024], P('tp'), may hold values from 1 to 15
- conv_gain: float32 [1024], P('tp'), may hold values from 0.1 to 1.9
- short_taps: bfloat16 [4, 1536], P(None, 'tp'), may hold values from -3 to 3
- decay_map: bfloat16 [24, 64, 64], P('tp'), may hold values from -0.75 to 0.75
- input_map: bfloat16 [24, 64, 64], P('tp'), may hold values from -0.75 to 0.75
- decay_base: float32 [1536], P('tp'), may hold values from 3.5 to 17
- decay_jump: float32 [6144, 1536], P('sp', 'tp'), may hold values from -1.5 to 0
- out_conv_w: bfloat16 [1024, 4096], P('tp', 'sp'), may hold values from -0.125 to 0.125
- out_rec_w: bfloat16 [1536, 4096], P('tp', 'sp'), may hold values from -0.125 to 0.125
Outputs:
- mixed: bfloat16 [6144, 4096], P(('sp', 'tp'))
All inputs are finite; a program needn't handle non-finite values.
Results may differ from a plain program's by a relative error of at most 0.015.
Values may be sent and summed in bfloat16 or wider, within the bound.
A program may use at most 128 MiB of HBM per device.

v0:
```python
import functools

import jax
import jax.numpy as jnp
from jax import lax
from jax.experimental import pallas as pl
from jax.experimental.pallas import tpu as pltpu
from jax.sharding import PartitionSpec as P

CONV_WIDTH = 1024


RATE_SCALE = 8.0


def passed_along(value, axis, by):
    count = lax.axis_size(axis)
    pairs = [(i, i + by) for i in range(count) if 0 <= i + by < count]
    return lax.ppermute(value, axis, pairs)


def prefix(part, axis, combine, identity):
    place = lax.axis_index(axis)
    gathered = jax.tree.map(lambda a: lax.all_gather(a, axis), part)
    state = jax.tree.map(lambda a, e: jnp.zeros_like(a) + jnp.asarray(e, a.dtype), part, identity)

    def one(step, state):
        return combine(
            state, jax.tree.map(lambda a: lax.dynamic_index_in_dim(a, step, 0, False), gathered)
        )

    return lax.fori_loop(0, place, one, state)


def norm_rows(values, gain):
    widened = values.astype(jnp.float32)
    inverse = lax.rsqrt(jnp.mean(widened * widened, axis=-1, keepdims=True) + 1e-06)
    return (widened * inverse * gain).astype(jnp.bfloat16)


def causal_window(edge, current, weights):
    extended = jnp.concatenate([edge, current], axis=0).astype(jnp.float32)
    taps_wide = weights.astype(jnp.float32)
    length = current.shape[0]
    result = jnp.zeros((length, current.shape[1]), jnp.float32)
    for lag_index in range(weights.shape[0]):
        result = result + taps_wide[lag_index][None, :] * extended[lag_index : lag_index + length]
    return result


def chain_step(earlier, latter):
    return (earlier[0] * latter[0], latter[0] * earlier[1] + latter[1])


def glu_of(conv_val, conv_gate):
    return (conv_val.astype(jnp.float32) * jax.nn.sigmoid(conv_gate.astype(jnp.float32))).astype(
        jnp.bfloat16
    )


def shards(
    tokens,
    norm_gain,
    conv_val_w,
    conv_gate_w,
    rec_gate_w,
    rec_in_w,
    conv_taps,
    conv_bias,
    conv_gain,
    short_taps,
    decay_map,
    input_map,
    decay_base,
    decay_jump,
    out_conv_w,
    out_rec_w,
):
    rec_cols = rec_in_w.shape[1]
    conv_lags = conv_taps.shape[0] - 1
    short_lags = short_taps.shape[0] - 1
    normed = norm_rows(tokens, norm_gain)
    val_full, gate_full = (
        lax.all_gather(conv_val_w, "sp", axis=0, tiled=True),
        lax.all_gather(conv_gate_w, "sp", axis=0, tiled=True),
    )
    all_rows = lax.all_gather(normed, "tp", axis=0, tiled=True)
    conv_val = jnp.dot(all_rows, val_full, preferred_element_type=jnp.float32).astype(jnp.bfloat16)
    conv_gate = jnp.dot(all_rows, gate_full, preferred_element_type=jnp.float32).astype(
        jnp.bfloat16
    )
    glu = glu_of(conv_val, conv_gate)
    conv_edge = passed_along(glu[-conv_lags:], "sp", 1)
    rgate_full, rin_full = (
        lax.all_gather(rec_gate_w, "sp", axis=0, tiled=True),
        lax.all_gather(rec_in_w, "sp", axis=0, tiled=True),
    )
    rec_gate = jnp.dot(all_rows, rgate_full, preferred_element_type=jnp.float32).astype(
        jnp.bfloat16
    )
    rec_in = jnp.dot(all_rows, rin_full, preferred_element_type=jnp.float32).astype(jnp.bfloat16)
    rec_edge = passed_along(rec_in[-short_lags:], "sp", 1)
    filtered = causal_window(conv_edge, glu, conv_taps) + conv_bias[None, :]
    row_total = lax.psum(jnp.sum(filtered, axis=1), "tp")
    centered = filtered - (row_total / CONV_WIDTH)[:, None]
    spread = lax.psum(jnp.sum(centered * centered, axis=1), "tp") / CONV_WIDTH
    conv_out = jax.nn.silu(centered * lax.rsqrt(spread + 1e-05)[:, None] * conv_gain).astype(
        jnp.bfloat16
    )
    smoothed = causal_window(rec_edge, rec_in, short_taps).astype(jnp.bfloat16)
    length = smoothed.shape[0]
    grouped = smoothed.reshape(length, decay_map.shape[0], decay_map.shape[1])
    retain = jax.nn.sigmoid(
        jnp.einsum("thi,hio->tho", grouped, decay_map, preferred_element_type=jnp.float32).reshape(
            length, rec_cols
        )
    )
    admit = jax.nn.sigmoid(
        jnp.einsum("thi,hio->tho", grouped, input_map, preferred_element_type=jnp.float32).reshape(
            length, rec_cols
        )
    )
    log_decay = -RATE_SCALE * retain * jax.nn.softplus(-decay_base)[None, :] + decay_jump
    decay = jnp.exp(log_decay)
    inflow = jnp.sqrt(-jnp.expm1(2.0 * log_decay)) * admit * smoothed.astype(jnp.float32)
    products, local_state = lax.associative_scan(chain_step, (decay, inflow), axis=0)
    entering = prefix(
        (products[-1], local_state[-1]),
        "sp",
        chain_step,
        (jnp.ones((rec_cols,), jnp.float32), jnp.zeros((rec_cols,), jnp.float32)),
    )
    state = local_state + products * entering[1][None, :]
    rec_out = (jax.nn.gelu(rec_gate.astype(jnp.float32)) * state).astype(jnp.bfloat16)
    conv_full, rec_full = (
        lax.all_gather(out_conv_w, "sp", axis=1, tiled=True),
        lax.all_gather(out_rec_w, "sp", axis=1, tiled=True),
    )
    return lax.psum_scatter(
        (
            jnp.dot(conv_out, conv_full, preferred_element_type=jnp.float32)
            + jnp.dot(rec_out, rec_full, preferred_element_type=jnp.float32)
        ).astype(jnp.bfloat16),
        "tp",
        scatter_dimension=0,
        tiled=True,
    )


MESH = pl.DeviceIdType.MESH
ANY = pl.BlockSpec(memory_space=pl.ANY)
VMEM = pl.BlockSpec(memory_space=pltpu.VMEM)
SEGMENTS = 8


class Spot:
    def __init__(self, planes):
        self.s, self.c = lax.axis_index("sp"), lax.axis_index("tp")
        self.z, self.q = self.s // 4, self.s % 4
        self.qx = self.q + 1 - 2 * (self.q % 2)
        self.qy = (self.q + 2) % 4
        self.qd = 3 - self.q
        self.has_up, self.has_down = self.z < planes - 1, self.z > 0
        self.up, self.down = self.at(self.s + 4, self.c), self.at(self.s - 4, self.c)
        self.partner = self.at(self.s, 1 - self.c)

    def at(self, s, c):
        return {"sp": s, "tp": c}

    def mate(self, q):
        return self.at(self.z * 4 + q, self.c)


class Mail:
    def __init__(self, send_sem):
        self.send_sem, self.count, self.open = send_sem, 0, []

    def send(self, src, dst, recv, device, when=None):
        copy = pltpu.make_async_remote_copy(
            src_ref=src, dst_ref=dst, send_sem=self.send_sem.at[self.count],
            recv_sem=recv, device_id=device, device_id_type=MESH,
        )
        self.count += 1
        self.open.append((copy.wait_send, when))
        if when is None:
            copy.start()
        else:
            pl.when(when)(copy.start)

    def local(self, src, dst):
        copy = pltpu.make_async_copy(src, dst, self.send_sem.at[self.count])
        self.count += 1
        copy.start()
        self.open.append((copy.wait, None))
        return self.open[-1]

    def arrived(self, dst, recv, device):
        pltpu.make_async_remote_copy(
            src_ref=dst, dst_ref=dst, send_sem=self.send_sem.at[0],
            recv_sem=recv, device_id=device, device_id_type=MESH,
        ).wait_recv()

    def finish(self):
        for wait, when in self.open:
            if when is None:
                wait()
            else:
                pl.when(when)(wait)


def greet(me, devices, line):
    barrier = pltpu.get_barrier_semaphore()
    for device in devices:
        pl.semaphore_signal(barrier, inc=1, device_id=device, device_id_type=MESH)
    amount = len(devices)
    if line:
        for has, device in ((me.has_up, me.up), (me.has_down, me.down)):
            @pl.when(has)
            def _():
                pl.semaphore_signal(barrier, inc=1, device_id=device, device_id_type=MESH)
        amount = amount + me.has_up.astype(jnp.int32) + me.has_down.astype(jnp.int32)
    pl.semaphore_wait(barrier, amount)


class PlaneGather:
    def __init__(self, me, mail, own, slot, recv, recv_pair):
        self.me, self.mail, self.own, self.slot = me, mail, own, slot
        self.recv, self.recv_pair = recv, recv_pair

    def start(self):
        me, mail = self.me, self.mail
        for h in (0, 1):
            for q, half in ((me.qx, h), (me.qy, 1 - h)):
                mail.send(self.own(half), self.slot(me.q, me.c, half), self.recv.at[me.q, half], me.mate(q))
        for half in (0, 1):
            mail.send(self.own(half), self.slot(me.q, me.c, half), self.recv_pair.at[me.q, half], me.partner)

    def took(self, q, half):
        me, mail = self.me, self.mail
        here = self.slot(q, me.c, half)
        mail.arrived(here, self.recv.at[q, half], me.partner)
        return here

    def share(self, q, half, here):
        self.mail.send(here, here, self.recv_pair.at[q, half], self.me.partner)

    def first(self):
        me = self.me
        for q, half, to in ((me.qx, 0, me.qy), (me.qy, 1, me.qx)):
            here = self.took(q, half)
            self.mail.send(here, here, self.recv.at[q, half], me.mate(to))
            self.share(q, half, here)

    def second(self):
        for q, half in ((self.me.qx, 1), (self.me.qy, 0)):
            self.share(q, half, self.took(q, half))

    def third(self):
        for half in (0, 1):
            self.share(self.me.qd, half, self.took(self.me.qd, half))

    def last(self):
        me = self.me
        for q in (me.q, me.qx, me.qy, me.qd):
            for half in (0, 1):
                self.mail.arrived(self.slot(q, 1 - me.c, half), self.recv_pair.at[q, half], me.partner)


def enter_kernel(
    planes, x_ref, gain, w_ref, j_ref, proj, jall, xall, wall, acc, send, rx, rp, rw, rz, rj
):
    me = Spot(planes)
    mail = Mail(send)
    greet(me, [me.mate(me.qx), me.mate(me.qy), me.mate(me.qd), me.partner], True)
    others = (me.qx, me.qy, me.qd)
    depth = w_ref.shape[1]
    rows = x_ref.shape[0]
    jwidth = j_ref.shape[1] // 4

    def wslot(origin, piece):
        return wall.at[pl.ds(pl.multiple_of((origin * 4 + piece) * depth, depth), depth)]

    def to_line(src, origin, piece):
        mail.send(src, wslot(origin, piece), rz.at[origin, piece], me.up, me.has_up)
        mail.send(src, wslot(origin, piece), rz.at[origin, piece], me.down, me.has_down)

    for q in others:
        mail.send(w_ref.at[q], wslot(me.z, me.q), rw.at[me.q], me.mate(q))
    to_line(w_ref.at[me.q], me.z, me.q)
    own_rows = mail.local(w_ref.at[me.q], wslot(me.z, me.q))

    first_row = (me.q * 2 + me.c) * rows

    @pl.loop(0, rows // 16)
    def _(i):
        values = x_ref[pl.ds(pl.multiple_of(i * 16, 16), 16)].astype(jnp.float32)
        inverse = lax.rsqrt(jnp.mean(values * values, axis=1, keepdims=True) + 1e-06)
        place = pl.ds(pl.multiple_of(first_row + i * 16, 16), 16)
        xall[place] = (values * inverse * gain[...]).astype(xall.dtype)

    half_rows = rows // 2

    def slot(q, c, h):
        return xall.at[pl.ds(pl.multiple_of((q * 2 + c) * rows + h * half_rows, 16), half_rows)]

    xg = PlaneGather(me, mail, lambda h: slot(me.q, me.c, h), slot, rx, rp)
    xg.start()
    for q in others:
        here = wslot(me.z, q)
        mail.arrived(here, rw.at[q], me.partner)
        to_line(here, me.z, q)

    def line_step(k):
        for piece in (me.q,) + others:
            for origin, there, on, more in (
                (me.z - k, me.z >= k, me.up, me.has_up),
                (me.z + k, me.z + k < planes, me.down, me.has_down),
            ):
                here = wslot(origin, piece)
                sem = rz.at[origin, piece]
                pl.when(there)(functools.partial(mail.arrived, here, sem, me.partner))
                mail.send(here, here, sem, on, jnp.logical_and(there, more))

    line_step(1)
    xg.first()

    def share(q):
        begin = q * jwidth // 128 * 128
        return j_ref.at[:, pl.ds(pl.multiple_of(begin, 128), jall.shape[2])]

    for q in others:
        mail.send(share(q), jall.at[me.q], rj.at[me.q], me.mate(q))
    mail.local(share(me.q), jall.at[me.q])
    for k in range(2, planes - 1):
        line_step(k)
    xg.second()
    xg.third()
    xg.last()
    mail.open.remove(own_rows)
    own_rows[0]()
    tile = acc.shape[0] // 4

    def multiply(start, size, fresh=False):
        at = pl.ds(pl.multiple_of(start, depth), size)

        @pl.loop(0, 4)
        def _(i):
            part = pl.ds(pl.multiple_of(i * tile, 16), tile)
            product = jnp.dot(xall[part, at], wall[at], preferred_element_type=jnp.float32)
            acc[part] = product if fresh else acc[part] + product

    multiply(me.z * 4 * depth, 4 * depth, True)
    for k in range(1, planes - 1):
        for origin, there in ((me.z - k, me.z >= k), (me.z + k, me.z + k < planes)):
            pl.when(there)(functools.partial(multiply, origin * 4 * depth, 4 * depth))
    far = planes - 1 - me.z

    @pl.when(jnp.logical_or(me.z == 0, me.z == planes - 1))
    def _():
        for piece in (me.q,) + others:
            mail.arrived(wslot(far, piece), rz.at[far, piece], me.partner)
            multiply((far * 4 + piece) * depth, depth)

    for q in others:
        mail.arrived(jall.at[q], rj.at[q], me.partner)
    mail.finish()

    @pl.loop(0, 8)
    def _(i):
        part = pl.ds(pl.multiple_of(i * (tile // 2), 16), tile // 2)
        proj[part] = acc[part].astype(proj.dtype)


def window_of(width):
    return max(-(-(q + 1) * width // 128) * 128 - q * width // 128 * 128 for q in range(4))


def enter(planes, tokens, gain, pieces, jumps):
    rows, width = tokens.shape
    depth, cols = pieces.shape[1:]
    dma, vmem = pltpu.SemaphoreType.DMA, pltpu.VMEM
    return pl.pallas_call(
        functools.partial(enter_kernel, planes),
        out_shape=(
            jax.ShapeDtypeStruct((8 * rows, cols), tokens.dtype),
            jax.ShapeDtypeStruct((4, jumps.shape[0], window_of(jumps.shape[1] // 4)), jumps.dtype),
        ),
        in_specs=[VMEM] * 4,
        out_specs=(VMEM,) * 2,
        scratch_shapes=[
            vmem((8 * rows, width), tokens.dtype),
            vmem((planes * 4 * depth, cols), pieces.dtype),
            vmem((8 * rows, cols), jnp.float32),
            dma((40 + 8 * planes,)), dma((4, 2)), dma((4, 2)), dma((4,)), dma((planes, 4)), dma((4,)),
        ],
        compiler_params=pltpu.CompilerParams(
            collective_id=0, has_side_effects=True, vmem_limit_bytes=56 * 1024 * 1024
        ),
    )(tokens, gain, pieces, jumps)


def minus_expm1(y):
    series = 1.0 + y * (1.0 / 8.0)
    for n in (7.0, 6.0, 5.0, 4.0, 3.0, 2.0):
        series = 1.0 + y * (1.0 / n) * series
    return jnp.where(y > -0.35, -y * series, 1.0 - jnp.exp(y))


def gelu(v):
    return 0.5 * v * (1.0 + jnp.tanh(0.7978845608028654 * (v + 0.044715 * v * v * v)))


def core_kernel(
    planes, lags, proj, jump, cpar, rpar, dmap, imap, w_ref,
    out, wz, wp, yall, cbuf, halo, gext, rext, filt, dec, inf, maps, stat, st_all, carry, cr_all,
    send, ry, rp, rv, rq, rz, rw, rh, rs, rc, ls, lr,
):
    me = Spot(planes)
    mail = Mail(send)
    c_lags, s_lags = lags
    f32, bf16 = jnp.float32, jnp.bfloat16
    length = proj.shape[0]
    cw = gext.shape[1]
    rwid = rpar.shape[2]
    seg = length // SEGMENTS
    top = halo.shape[0]
    fold = dec.shape[0]
    part = planes // 2
    width = yall.shape[1] // 8
    mine = me.q * 2 + me.c
    mates = [me.at(me.z * 4 + (me.q + dq) % 4, c) for dq in range(4) for c in (me.c, 1 - me.c)][1:]
    lined = [me.at((me.s + 4 * k) % (4 * planes), me.c) for k in range(1, planes)]
    greet(me, mates + lined, False)

    def hand_over(src, origin, when):
        theirs = origin // part != me.c
        if when is not None:
            theirs = jnp.logical_and(theirs, when)
        place = origin - (1 - me.c) * part
        mail.send(src, wp.at[place], rw.at[place], me.partner, theirs)

    mail.send(proj.at[pl.ds(length - top, top)], halo, rh.at[0], me.up, me.has_up)
    mail.send(w_ref, wz.at[me.z], rz.at[me.z], me.up, me.has_up)
    mail.send(w_ref, wz.at[me.z], rz.at[me.z], me.down, me.has_down)
    hand_over(w_ref, me.z, None)
    mail.local(w_ref, wz.at[me.z])

    maps[...] = jnp.zeros_like(maps)
    size = dmap.shape[1]
    heads = rwid // size
    for h in range(heads):
        spot = pl.ds(h * size, size)
        maps[spot, pl.ds(h * size, size)] = dmap[me.q * heads + h]
        maps[spot, pl.ds(fold * 128 + h * size, size)] = imap[me.q * heads + h]

    def columns(ref, row, count):
        val = ref[pl.ds(row, count), pl.ds(0, cw)].astype(f32)
        gate = ref[pl.ds(row, count), pl.ds(cw, cw)].astype(f32)
        return (val * jax.nn.sigmoid(gate)).astype(bf16).astype(f32)

    rec_at, gate_at = 2 * cw + rwid, 2 * cw

    @pl.loop(0, SEGMENTS)
    def _(i):
        base = pl.multiple_of(i * seg, 16)
        rext[pl.ds(pl.multiple_of(base + top, 8), seg)] = proj[pl.ds(base, seg), pl.ds(rec_at, rwid)].astype(f32)

    @pl.when(me.has_down)
    def _():
        mail.arrived(halo, rh.at[0], me.partner)
        rext[pl.ds(0, top)] = halo[:, pl.ds(rec_at, rwid)].astype(f32)

    @pl.when(jnp.logical_not(me.has_down))
    def _():
        rext[pl.ds(0, top)] = jnp.zeros((top, rwid), f32)

    softened = rpar[me.q, pl.ds(s_lags + 1, 1), :]

    @pl.loop(0, SEGMENTS)
    def _(i):
        base = pl.multiple_of(i * seg, 8)
        window = rext[pl.ds(pl.multiple_of(base + top - 8, 8), seg + 8)]
        smooth = jnp.zeros((seg, rwid), f32)
        for k in range(s_lags + 1):
            smooth = smooth + rpar[me.q, pl.ds(k, 1), :] * window[8 - s_lags + k : 8 - s_lags + k + seg]
        smooth = smooth.astype(bf16)
        gates = jax.nn.sigmoid(jnp.dot(smooth, maps[...], preferred_element_type=f32))
        retain, admit = gates[:, :rwid], gates[:, fold * 128 : fold * 128 + rwid]
        wide = jump[pl.ds(base, seg)]
        moved = wide[:, :rwid]
        for lead in {q * rwid % 128 for q in range(4)} - {0}:
            moved = jnp.where(me.q * rwid % 128 == lead, wide[:, lead : lead + rwid], moved)
        log_decay = moved - retain * softened
        decay = jnp.exp(log_decay)
        inflow = jnp.sqrt(minus_expm1(2.0 * log_decay)) * admit * smooth.astype(f32)
        for f in range(fold):
            w = min(128, rwid - f * 128)
            dec[f, pl.ds(base, seg), pl.ds(0, w)] = decay[:, f * 128 : f * 128 + w]
            inf[f, pl.ds(base, seg), pl.ds(0, w)] = inflow[:, f * 128 : f * 128 + w]

    def one(i, held):
        after = []
        for f in range(fold):
            at = pl.ds(i, SEGMENTS, stride=seg)
            d = dec.at[f][at, :]
            product, state = held[2 * f] * d, held[2 * f + 1] * d + inf.at[f][at, :]
            dec.at[f][at, :] = product
            inf.at[f][at, :] = state
            after += [product, state]
        return tuple(after)

    flat = (SEGMENTS, 128)
    ends = lax.fori_loop(0, seg, one, (jnp.ones(flat, f32), jnp.zeros(flat, f32)) * fold, unroll=8)
    for f in range(fold):
        product, state = jnp.ones((1, 128), f32), jnp.zeros((1, 128), f32)
        for i in range(SEGMENTS):
            p, s = ends[2 * f][i : i + 1], ends[2 * f + 1][i : i + 1]
            product, state = product * p, p * state + s
        carry[pl.ds(2 * f, 1)] = product
        carry[pl.ds(2 * f + 1, 1)] = state
    for device in lined:
        mail.send(carry, cr_all.at[me.z], rc.at[me.z], device)

    @pl.loop(0, SEGMENTS)
    def _(i):
        base = pl.multiple_of(i * seg, 16)
        gext[pl.ds(pl.multiple_of(base + top, 8), seg)] = columns(proj, base, seg)

    @pl.when(me.has_down)
    def _():
        gext[pl.ds(0, top)] = columns(halo, 0, top)

    @pl.when(jnp.logical_not(me.has_down))
    def _():
        gext[pl.ds(0, top)] = jnp.zeros((top, cw), f32)

    def line_step(k):
        for origin, there, on, more in (
            (me.z - k, me.z >= k, me.up, me.has_up),
            (me.z + k, me.z + k < planes, me.down, me.has_down),
        ):
            pl.when(there)(functools.partial(mail.arrived, wz.at[origin], rz.at[origin], me.partner))
            if k < planes - 1:
                mail.send(wz.at[origin], wz.at[origin], rz.at[origin], on, jnp.logical_and(there, more))
            hand_over(wz.at[origin], origin, there)

    for k in range(1, planes):
        z = (me.z + k) % planes
        mail.arrived(cr_all.at[z], rc.at[z], me.partner)
    cr_all[me.z] = carry[...]
    entering = []
    for f in range(fold):
        held = jnp.zeros((1, 128), f32)
        for j in range(planes - 1):
            after = cr_all[j, pl.ds(2 * f, 1)] * held + cr_all[j, pl.ds(2 * f + 1, 1)]
            held = jnp.where(j < me.z, after, held)
        for i in range(SEGMENTS):
            entering.append(held)
            held = ends[2 * f][i : i + 1] * held + ends[2 * f + 1][i : i + 1]
    own_at = pl.multiple_of(mine * width, 128)
    for i in range(SEGMENTS):
        rows = pl.ds(i * seg, seg)
        state = [dec[f, rows] * entering[f * SEGMENTS + i] + inf[f, rows] for f in range(fold)]
        state = jnp.concatenate(state, axis=1)[:, :rwid]
        result = gelu(proj[rows, pl.ds(gate_at, rwid)].astype(f32)) * state
        fill = jnp.zeros((seg, width - cw - rwid), f32)
        yall[rows, pl.ds(pl.multiple_of(own_at + cw, 128), width - cw)] = jnp.concatenate([result, fill], axis=1).astype(bf16)

    half_rows = length // 2

    def gather(lane, lanes, recv, recv_pair):
        def slot(q, c, h):
            spot = pl.ds(pl.multiple_of((q * 2 + c) * width + lane, 128), lanes)
            return yall.at[pl.ds(h * half_rows, half_rows), spot]

        return PlaneGather(me, mail, lambda h: slot(me.q, me.c, h), slot, recv, recv_pair)

    vg = gather(cw, width - cw, rv, rq)
    vg.start()

    @pl.loop(0, length // 64)
    def _(i):
        base = pl.multiple_of(i * 64, 8)
        window = gext[pl.ds(base, 64 + top)]
        total = jnp.zeros((64, cw), f32) + cpar[pl.ds(c_lags + 1, 1), :]
        for k in range(c_lags + 1):
            begin = top - c_lags + k
            total = total + cpar[pl.ds(k, 1), :] * window[begin : begin + 64]
        filt[pl.ds(base, 64)] = total
        part_sum = jnp.sum(total, axis=1, keepdims=True)
        off = total - part_sum * (1.0 / cw)
        lane = lax.broadcasted_iota(jnp.int32, (64, 128), 1)
        spread = jnp.sum(off * off, axis=1, keepdims=True)
        stat[pl.ds(base, 64)] = jnp.where(lane == 0, part_sum, spread)

    packed = stat[...].T
    st_all[mine] = packed[0:8]
    for device in mates:
        mail.send(st_all.at[mine], st_all.at[mine], rs.at[mine], device)

    line_step(1)
    for k in range(1, 8):
        d = (mine + k) % 8
        mail.arrived(st_all.at[d], rs.at[d], me.partner)
    total = sum(st_all[d, 0:1, :] for d in range(8))
    mean = total * (1.0 / (8 * cw))
    spread = jnp.zeros_like(mean)
    for d in range(8):
        shift = st_all[d, 0:1, :] * (1.0 / cw) - mean
        spread = spread + st_all[d, 1:2, :] + cw * shift * shift
    scale = lax.rsqrt(spread * (1.0 / (8 * cw)) + 1e-05)
    row = lax.broadcasted_iota(jnp.int32, (128, length), 0)
    stat[...] = jnp.where(row == 0, mean, scale).T

    @pl.loop(0, SEGMENTS)
    def _(i):
        rows = pl.ds(pl.multiple_of(i * seg, 16), seg)
        pair = stat[rows]
        v = (filt[rows] - pair[:, 0:1]) * pair[:, 1:2] * cpar[pl.ds(c_lags + 2, 1), :]
        yall[rows, pl.ds(own_at, cw)] = (v * jax.nn.sigmoid(v)).astype(bf16)

    yg = gather(0, cw, ry, rp)
    yg.start()
    vg.first()
    yg.first()
    for k in range(2, planes - 1):
        line_step(k)
    vg.second()
    yg.second()
    vg.third()
    yg.third()
    line_step(planes - 1)
    for k in range(part):
        mail.arrived(wp.at[k], rw.at[k], me.partner)
    vg.last()
    yg.last()
    mail.finish()

    used, cols = cw + rwid, w_ref.shape[1]
    tile = length // 8

    def multiply(d):
        rows = pl.ds(pl.multiple_of(d * tile, 16), tile)
        for k in range(part):
            total = jnp.zeros((tile, cols), f32)
            for q in range(4):
                for c, block in ((me.c, wz.at[me.c * part + k]), (1 - me.c, wp.at[k])):
                    left = yall[rows, pl.ds(pl.multiple_of((q * 2 + c) * width, 128), width)]
                    total = total + jnp.dot(
                        left[:, :used], block[pl.ds(q * used, used)], preferred_element_type=f32
                    )
            cbuf[d, k] = total.astype(bf16)

    def place(q, c, k):
        return out.at[:, pl.ds(pl.multiple_of(((c * part + k) * 4 + q) * cols, 128), cols)]

    def target(i):
        flip = 3 - i // 2
        q = (me.q // 2 + flip // 2) % 2 * 2 + (me.q % 2 + flip % 2) % 2
        return q, (me.c + 1 + i) % 2

    def parcel(i, k):
        q, c = target(i)
        return pltpu.make_async_remote_copy(
            src_ref=cbuf.at[q * 2 + c, k], dst_ref=place(me.q, me.c, k), send_sem=ls.at[i, k],
            recv_sem=lr.at[mine, k], device_id=me.at(me.z * 4 + q, c), device_id_type=MESH,
        )

    @pl.loop(0, 7)
    def _(i):
        q, c = target(i)
        multiply(q * 2 + c)
        for k in range(part):
            parcel(i, k).start()

    multiply(mine)
    kept = [pltpu.make_async_copy(cbuf.at[mine, k], place(me.q, me.c, k), ls.at[7, k]) for k in range(part)]
    for copy in kept:
        copy.start()

    @pl.loop(0, 7)
    def _(i):
        q, c = target(i)
        for k in range(part):
            mail.arrived(place(q, c, k), lr.at[q * 2 + c, k], me.partner)
            parcel(i, k).wait_send()

    for copy in kept:
        copy.wait()


def core(planes, proj, jump, cpar, rpar, dmap, imap, weights, lags, cw):
    length, rwid = jump.shape[0], rpar.shape[2]
    used, cols = cw + rwid, weights.shape[1]
    width = used + -used % 128
    fold = (rwid + 127) // 128
    f32, bf16 = jnp.float32, jnp.bfloat16
    dma, vmem = pltpu.SemaphoreType.DMA, pltpu.VMEM
    top = lags[0] + -lags[0] % 16
    part = planes // 2
    return pl.pallas_call(
        functools.partial(core_kernel, planes, lags),
        out_shape=jax.ShapeDtypeStruct((length // 8, planes * 4 * cols), bf16),
        in_specs=[VMEM] * 7,
        out_specs=ANY,
        scratch_shapes=[
            vmem((planes,) + weights.shape, bf16),
            vmem((part,) + weights.shape, bf16),
            vmem((length, 8 * width), bf16),
            vmem((8, part, length // 8, cols), bf16),
            vmem((top, proj.shape[1]), bf16),
            vmem((top + length, cw), f32),
            vmem((top + length, rwid), f32),
            vmem((length, cw), f32),
            vmem((fold, length, 128), f32),
            vmem((fold, length, 128), f32),
            vmem((rwid, 2 * fold * 128), bf16),
            vmem((length, 128), f32),
            vmem((8, 8, length), f32),
            vmem((8, 128), f32),
            vmem((planes, 8, 128), f32),
            dma((64 + 8 * planes,)), dma((4, 2)), dma((4, 2)), dma((4, 2)), dma((4, 2)), dma((planes,)), dma((part,)),
            dma((1,)), dma((8,)), dma((planes,)), dma((8, part)), dma((8, part)),
        ],
        compiler_params=pltpu.CompilerParams(
            collective_id=2, has_side_effects=True, vmem_limit_bytes=60 * 1024 * 1024
        ),
    )(proj, jump, cpar, rpar, dmap, imap, weights)


def plane_shards(
    planes,
    tokens,
    norm_gain,
    conv_val_w,
    conv_gate_w,
    rec_gate_w,
    rec_in_w,
    conv_taps,
    conv_bias,
    conv_gain,
    short_taps,
    decay_map,
    input_map,
    decay_base,
    decay_jump,
    out_conv_w,
    out_rec_w,
):
    s = lax.axis_index("sp")
    q = s % 4
    f32 = jnp.float32

    def by_mate(a):
        return a.reshape(a.shape[0], 4, a.shape[1] // 4).transpose(1, 0, 2)

    def mine(a, axis):
        size = a.shape[axis] // 4
        return lax.dynamic_slice_in_dim(a, q * size, size, axis)

    pieces = jnp.concatenate([by_mate(w) for w in (conv_val_w, conv_gate_w, rec_gate_w, rec_in_w)], axis=2)
    projected, jall = enter(planes, tokens, norm_gain[None], pieces, decay_jump)
    cw, rw = conv_val_w.shape[1] // 4, rec_in_w.shape[1] // 4
    jump = jall.reshape(-1, jall.shape[2])
    cols = out_conv_w.shape[1]
    rows_by_mate = jnp.concatenate(
        [out_conv_w.reshape(4, cw, cols), out_rec_w.reshape(4, rw, cols)], axis=1
    ).reshape(-1, cols)
    cpar = mine(jnp.concatenate([conv_taps.astype(f32), conv_bias[None], conv_gain[None]]), 1)
    rpar = by_mate(jnp.concatenate([short_taps.astype(f32), RATE_SCALE * jax.nn.softplus(-decay_base)[None]]))
    lags = (conv_taps.shape[0] - 1, short_taps.shape[0] - 1)
    return core(planes, projected, jump, cpar, rpar, decay_map, input_map, rows_by_mate, lags, cw)


def solution(mesh):
    in_specs = (
        P(("sp", "tp"), None),
        P(),
        P("sp", "tp"),
        P("sp", "tp"),
        P("sp", "tp"),
        P("sp", "tp"),
        P(None, "tp"),
        P("tp"),
        P("tp"),
        P(None, "tp"),
        P("tp", None, None),
        P("tp", None, None),
        P("tp"),
        P("sp", "tp"),
        P("tp", "sp"),
        P("tp", "sp"),
    )
    out_specs = P(("sp", "tp"), None)
    count = mesh.shape["sp"]
    planar = mesh.shape["tp"] == 2 and count % 8 == 0 and count >= 16
    body = functools.partial(plane_shards, count // 4) if planar else shards
    return jax.shard_map(body, mesh=mesh, in_specs=in_specs, out_specs=out_specs, check_vma=False)
```

profile of v0, /device:TPU:0, one launch (start us, length us, event | category | flops | bytes accessed | tf_op | source)
XLA Modules:
  0.0 203.0 jit_solution(17425261352360337828)
XLA Ops:
  0.0 0.0 copy-start
  0.0 0.0 copy-start.4
  0.0 0.8 fusion.2
  0.8 0.1 concatenate.23
  0.9 0.8 reshape.38
  1.6 0.6 maximum_bitcast_fusion.rpar
  2.3 0.8 convert_element_type.4
  3.0 1.3 fusion.1.cpar
  4.4 1.1 copy.17
  5.5 0.0 copy-start.1
  5.5 0.2 copy.18
  5.6 0.0 copy-done.4
  5.7 0.1 copy.19
  5.8 0.2 copy.20
  6.0 0.0 copy-done
  6.0 0.2 copy.21
  6.2 0.2 copy.22
  6.4 0.1 copy-done.1
  6.5 0.2 copy.23
  6.6 0.2 copy.24
  6.8 0.0 copy-start.2
  6.9 0.0 copy-start.3
  6.9 1.4 pad_maximum_fusion.w_ref
  8.2 0.0 copy-done.2
  8.2 0.0 copy-done.3
  8.2 0.9 pad_maximum_fusion.1
  9.1 97.1 %shard_map.154 = (bf16[1536,640]{1,0:T(8,128)(2,1)}, f32[4,384,256]{2,1,0:T(8,128)}) custom-call(bf16[192,4096]{1,0:T(8,128)(2,1)} %x_ref.1, f32[1,4096]{1,0:T(1,128)} %bitcast.29, bf16[4,256,640]{2,1,0:T(8,128)(2,1)} %pad_maximum_fusion.w_ref, f32[384,768]{1,0:T(8,128)} %j_ref.1), custom_call_target="tpu_custom_call" | custom-call | tf_op jit(solution)/shard_map/pallas_call | solution.py:382
  106.3 94.0 %shard_map.155 = bf16[192,4096]{1,0:T(8,128)(2,1)} custom-call(bf16[1536,640]{1,0:T(8,128)(2,1)} %get-tuple-element.7.proj, f32[1536,256]{1,0:T(8,128)} %bitcast.22, f32[33,128]{1,0:T(8,128)} %fusion.1.cpar, f32[4,5,192]{2,1,0:T(8,128)} %maximum_bitcast_fusion.rpar, bf16[12,64,64]{2,1,0:T(8,128)(2,1)} %dmap.1, bf16[12,64,64]{2,1,0:T(8,128)(2,1)} %imap.1, ...), custom_call_target="tpu_custom_call" | custom-call | tf_op jit(solution)/shard_map/pallas_call | solution.py:701
  200.3 2.7 %copy.27 = bf16[192,4096]{1,0:T(8,128)(2,1)} copy(bf16[192,4096]{1,0:T(8,128)(2,1)} %shard_map.155) | data formatting | bytes 3145728
  (1 shorter events, 0.0 us)
Async XLA Ops:
  0.0 6.0 %copy-start = (bf16[256,768]{1,0:T(8,128)(2,1)S(1)}, bf16[256,768]{1,0:T(8,128)(2,1)}, u32[]{:S(2)}) copy-start(bf16[256,768]{1,0:T(8,128)(2,1)} %param.20) | copy-start | bytes 1179652
  0.0 5.6 %copy-start.4 = (bf16[256,512]{1,0:T(8,128)(2,1)S(1)}, bf16[256,512]{1,0:T(8,128)(2,1)}, u32[]{:S(2)}) copy-start(bf16[256,512]{1,0:T(8,128)(2,1)} %param.19) | copy-start | bytes 786436
  5.5 1.0 copy-start.1
  6.8 1.4 copy-start.2
  6.9 1.4 copy-start.3
where the time goes:
time: 203 us
  Pallas kernels  191 us (94%)
  local copies, waits for them, and re-layouts  5.99 us (3%)
  other arithmetic  5.76 us (3%)
    pallas_call x1, Pallas kernels, enter(): pl.pallas_call(functools.partial(enter_kernel, planes), out_shape=(jax.Sh...  97.1 us
    pallas_call x1, Pallas kernels, core(): pl.pallas_call(functools.partial(core_kernel, planes, lags), out_shape=ja...  94 us
    unnamed x15, local copies, waits for them, and re-layouts  4.37 us

commit v1 on v0

--- a/solution.py
+++ b/solution.py
@@ -259,144 +259,11 @@
         for half in (0, 1):
             self.share(self.me.qd, half, self.took(self.me.qd, half))
 
-    def last(self):
+    def last(self, origins):
         me = self.me
-        for q in (me.q, me.qx, me.qy, me.qd):
+        for q in origins:
             for half in (0, 1):
                 self.mail.arrived(self.slot(q, 1 - me.c, half), self.recv_pair.at[q, half], me.partner)
-
-
-def enter_kernel(
-    planes, x_ref, gain, w_ref, j_ref, proj, jall, xall, wall, acc, send, rx, rp, rw, rz, rj
-):
-    me = Spot(planes)
-    mail = Mail(send)
-    greet(me, [me.mate(me.qx), me.mate(me.qy), me.mate(me.qd), me.partner], True)
-    others = (me.qx, me.qy, me.qd)
-    depth = w_ref.shape[1]
-    rows = x_ref.shape[0]
-    jwidth = j_ref.shape[1] // 4
-
-    def wslot(origin, piece):
-        return wall.at[pl.ds(pl.multiple_of((origin * 4 + piece) * depth, depth), depth)]
-
-    def to_line(src, origin, piece):
-        mail.send(src, wslot(origin, piece), rz.at[origin, piece], me.up, me.has_up)
-        mail.send(src, wslot(origin, piece), rz.at[origin, piece], me.down, me.has_down)
-
-    for q in others:
-        mail.send(w_ref.at[q], wslot(me.z, me.q), rw.at[me.q], me.mate(q))
-    to_line(w_ref.at[me.q], me.z, me.q)
-    own_rows = mail.local(w_ref.at[me.q], wslot(me.z, me.q))
-
-    first_row = (me.q * 2 + me.c) * rows
-
-    @pl.loop(0, rows // 16)
-    def _(i):
-        values = x_ref[pl.ds(pl.multiple_of(i * 16, 16), 16)].astype(jnp.float32)
-        inverse = lax.rsqrt(jnp.mean(values * values, axis=1, keepdims=True) + 1e-06)
-        place = pl.ds(pl.multiple_of(first_row + i * 16, 16), 16)
-        xall[place] = (values * inverse * gain[...]).astype(xall.dtype)
-
-    half_rows = rows // 2
-
-    def slot(q, c, h):
-        return xall.at[pl.ds(pl.multiple_of((q * 2 + c) * rows + h * half_rows, 16), half_rows)]
-
-    xg = PlaneGather(me, mail, lambda h: slot(me.q, me.c, h), slot, rx, rp)
-    xg.start()
-    for q in others:
-        here = wslot(me.z, q)
-        mail.arrived(here, rw.at[q], me.partner)
-        to_line(here, me.z, q)
-
-    def line_step(k):
-        for piece in (me.q,) + others:
-            for origin, there, on, more in (
-                (me.z - k, me.z >= k, me.up, me.has_up),
-                (me.z + k, me.z + k < planes, me.down, me.has_down),
-            ):
-                here = wslot(origin, piece)
-                sem = rz.at[origin, piece]
-                pl.when(there)(functools.partial(mail.arrived, here, sem, me.partner))
-                mail.send(here, here, sem, on, jnp.logical_and(there, more))
-
-    line_step(1)
-    xg.first()
-
-    def share(q):
-        begin = q * jwidth // 128 * 128
-        return j_ref.at[:, pl.ds(pl.multiple_of(begin, 128), jall.shape[2])]
-
-    for q in others:
-        mail.send(share(q), jall.at[me.q], rj.at[me.q], me.mate(q))
-    mail.local(share(me.q), jall.at[me.q])
-    for k in range(2, planes - 1):
-        line_step(k)
-    xg.second()
-    xg.third()
-    xg.last()
-    mail.open.remove(own_rows)
-    own_rows[0]()
-    tile = acc.shape[0] // 4
-
-    def multiply(start, size, fresh=False):
-        at = pl.ds(pl.multiple_of(start, depth), size)
-
-        @pl.loop(0, 4)
-        def _(i):
-            part = pl.ds(pl.multiple_of(i * tile, 16), tile)
-            product = jnp.dot(xall[part, at], wall[at], preferred_element_type=jnp.float32)
-            acc[part] = product if fresh else acc[part] + product
-
-    multiply(me.z * 4 * depth, 4 * depth, True)
-    for k in range(1, planes - 1):
-        for origin, there in ((me.z - k, me.z >= k), (me.z + k, me.z + k < planes)):
-            pl.when(there)(functools.partial(multiply, origin * 4 * depth, 4 * depth))
-    far = planes - 1 - me.z
-
-    @pl.when(jnp.logical_or(me.z == 0, me.z == planes - 1))
-    def _():
-        for piece in (me.q,) + others:
-            mail.arrived(wslot(far, piece), rz.at[far, piece], me.partner)
-            multiply((far * 4 + piece) * depth, depth)
-
-    for q in others:
-        mail.arrived(jall.at[q], rj.at[q], me.partner)
-    mail.finish()
-
-    @pl.loop(0, 8)
-    def _(i):
-        part = pl.ds(pl.multiple_of(i * (tile // 2), 16), tile // 2)
-        proj[part] = acc[part].astype(proj.dtype)
-
-
-def window_of(width):
-    return max(-(-(q + 1) * width // 128) * 128 - q * width // 128 * 128 for q in range(4))
-
-
-def enter(planes, tokens, gain, pieces, jumps):
-    rows, width = tokens.shape
-    depth, cols = pieces.shape[1:]
-    dma, vmem = pltpu.SemaphoreType.DMA, pltpu.VMEM
-    return pl.pallas_call(
-        functools.partial(enter_kernel, planes),
-        out_shape=(
-            jax.ShapeDtypeStruct((8 * rows, cols), tokens.dtype),
-            jax.ShapeDtypeStruct((4, jumps.shape[0], window_of(jumps.shape[1] // 4)), jumps.dtype),
-        ),
-        in_specs=[VMEM] * 4,
-        out_specs=(VMEM,) * 2,
-        scratch_shapes=[
-            vmem((8 * rows, width), tokens.dtype),
-            vmem((planes * 4 * depth, cols), pieces.dtype),
-            vmem((8 * rows, cols), jnp.float32),
-            dma((40 + 8 * planes,)), dma((4, 2)), dma((4, 2)), dma((4,)), dma((planes, 4)), dma((4,)),
-        ],
-        compiler_params=pltpu.CompilerParams(
-            collective_id=0, has_side_effects=True, vmem_limit_bytes=56 * 1024 * 1024
-        ),
-    )(tokens, gain, pieces, jumps)
 
 
 def minus_expm1(y):
@@ -410,40 +277,119 @@
     return 0.5 * v * (1.0 + jnp.tanh(0.7978845608028654 * (v + 0.044715 * v * v * v)))
 
 
-def core_kernel(
-    planes, lags, proj, jump, cpar, rpar, dmap, imap, w_ref,
-    out, wz, wp, yall, cbuf, halo, gext, rext, filt, dec, inf, maps, stat, st_all, carry, cr_all,
-    send, ry, rp, rv, rq, rz, rw, rh, rs, rc, ls, lr,
+class Line:
+    def __init__(self, me, mail, planes, slot, recv, seen=None):
+        self.me, self.mail, self.planes = me, mail, planes
+        self.slot, self.recv, self.seen = slot, recv, seen
+
+    def own(self, piece, src, up=True, down=True):
+        me = self.me
+        for wanted, has, device in ((up, me.has_up, me.up), (down, me.has_down, me.down)):
+            if wanted:
+                self.mail.send(src, self.slot(me.z, piece), self.recv.at[me.z, piece], device, has)
+
+    def relay(self, k, piece, up=True, down=True):
+        me = self.me
+        for wanted, origin, there, on, more in (
+            (up, me.z - k, me.z >= k, me.up, me.has_up),
+            (down, me.z + k, me.z + k < self.planes, me.down, me.has_down),
+        ):
+            if wanted:
+                here, sem = self.slot(origin, piece), self.recv.at[origin, piece]
+                pl.when(there)(functools.partial(self.mail.arrived, here, sem, me.partner))
+                if k < self.planes - 1:
+                    self.mail.send(here, here, sem, on, jnp.logical_and(there, more))
+                if self.seen is not None:
+                    self.seen(origin, piece, there)
+
+
+OUT_PARTS = 4
+
+
+def layer_kernel(
+    planes, lags, x_ref, gain, wr, wc, jb, cpar, rpar, dmap, imap, w_ref,
+    out, xall, rwall, cwall, projr, jall, wz, wp, yall, cbuf, gext, rext, filt, dec, inf, maps, stat,
+    st_all, carry, cr_all,
+    send, rx, rpx, rwr, rwc, zr, zc, zo, rj, ry, rp, rv, rq, rw, rh, rs, rc, ls, lr,
 ):
     me = Spot(planes)
     mail = Mail(send)
     c_lags, s_lags = lags
     f32, bf16 = jnp.float32, jnp.bfloat16
-    length = proj.shape[0]
-    cw = gext.shape[1]
-    rwid = rpar.shape[2]
+    rows, depth = x_ref.shape[0], wr.shape[1]
+    length = xall.shape[0]
+    cw, rwid = gext.shape[1], rpar.shape[2]
     seg = length // SEGMENTS
-    top = halo.shape[0]
+    top = gext.shape[0] - length
+    rtop = rext.shape[0] - length
     fold = dec.shape[0]
     part = planes // 2
     width = yall.shape[1] // 8
     mine = me.q * 2 + me.c
+    others = (me.qx, me.qy, me.qd)
+    pieces = (me.q,) + others
+    parts = tuple(range(OUT_PARTS))
+    tall = w_ref.shape[0] // OUT_PARTS
+    last = planes - 1
     mates = [me.at(me.z * 4 + (me.q + dq) % 4, c) for dq in range(4) for c in (me.c, 1 - me.c)][1:]
     lined = [me.at((me.s + 4 * k) % (4 * planes), me.c) for k in range(1, planes)]
     greet(me, mates + lined, False)
 
-    def hand_over(src, origin, when):
-        theirs = origin // part != me.c
-        if when is not None:
-            theirs = jnp.logical_and(theirs, when)
+    def of_rows(ref):
+        def slot(origin, piece):
+            return ref.at[pl.ds(pl.multiple_of((origin * 4 + piece) * depth, depth), depth)]
+
+        return slot
+
+    def theirs_too(origin, piece, when):
+        theirs = jnp.logical_and(origin // part != me.c, when)
         place = origin - (1 - me.c) * part
-        mail.send(src, wp.at[place], rw.at[place], me.partner, theirs)
-
-    mail.send(proj.at[pl.ds(length - top, top)], halo, rh.at[0], me.up, me.has_up)
-    mail.send(w_ref, wz.at[me.z], rz.at[me.z], me.up, me.has_up)
-    mail.send(w_ref, wz.at[me.z], rz.at[me.z], me.down, me.has_down)
-    hand_over(w_ref, me.z, None)
-    mail.local(w_ref, wz.at[me.z])
+        rest = pl.ds(piece * tall, tall)
+        mail.send(wz.at[origin, rest], wp.at[place, rest], rw.at[place, piece], me.partner, theirs)
+
+    rl = Line(me, mail, planes, of_rows(rwall), zr)
+    cl = Line(me, mail, planes, of_rows(cwall), zc)
+    ol = Line(me, mail, planes, lambda origin, p: wz.at[origin, pl.ds(p * tall, tall)], zo, theirs_too)
+
+    def out_own(p):
+        ol.own(p, w_ref.at[pl.ds(p * tall, tall)])
+
+    for q in others:
+        mail.send(wr.at[q], rl.slot(me.z, me.q), rwr.at[me.q], me.mate(q))
+    rl.own(me.q, wr.at[me.q])
+
+    first_row = mine * rows
+
+    @pl.loop(0, rows // 16)
+    def _(i):
+        values = x_ref[pl.ds(pl.multiple_of(i * 16, 16), 16)].astype(f32)
+        inverse = lax.rsqrt(jnp.mean(values * values, axis=1, keepdims=True) + 1e-06)
+        place = pl.ds(pl.multiple_of(first_row + i * 16, 16), 16)
+        xall[place] = (values * inverse * gain[...]).astype(bf16)
+
+    half_rows = rows // 2
+
+    def xslot(q, c, h):
+        return xall.at[pl.ds(pl.multiple_of((q * 2 + c) * rows + h * half_rows, 16), half_rows)]
+
+    xg = PlaneGather(me, mail, lambda h: xslot(me.q, me.c, h), xslot, rx, rpx)
+    xg.start()
+    for q in others:
+        mail.send(wc.at[q], cl.slot(me.z, me.q), rwc.at[me.q], me.mate(q))
+    out_own(0)
+    kept_here = [
+        mail.local(wr.at[me.q], rl.slot(me.z, me.q)),
+        mail.local(wc.at[me.q], cl.slot(me.z, me.q)),
+        mail.local(w_ref, wz.at[me.z]),
+        mail.local(jb.at[me.q], jall.at[me.q]),
+    ]
+    for entry in kept_here:
+        mail.open.remove(entry)
+        entry[0]()
+    for p in parts:
+        rest = pl.ds(p * tall, tall)
+        place = me.z - (1 - me.c) * part
+        mail.send(w_ref.at[rest], wp.at[place, rest], rw.at[place, p], me.partner, me.z // part != me.c)
 
     maps[...] = jnp.zeros_like(maps)
     size = dmap.shape[1]
@@ -453,43 +399,81 @@
         maps[spot, pl.ds(h * size, size)] = dmap[me.q * heads + h]
         maps[spot, pl.ds(fold * 128 + h * size, size)] = imap[me.q * heads + h]
 
-    def columns(ref, row, count):
-        val = ref[pl.ds(row, count), pl.ds(0, cw)].astype(f32)
-        gate = ref[pl.ds(row, count), pl.ds(cw, cw)].astype(f32)
-        return (val * jax.nn.sigmoid(gate)).astype(bf16).astype(f32)
-
-    rec_at, gate_at = 2 * cw + rwid, 2 * cw
-
-    @pl.loop(0, SEGMENTS)
+    for q in others:
+        here = rl.slot(me.z, q)
+        mail.arrived(here, rwr.at[q], me.partner)
+        rl.own(q, here)
+    for p in pieces:
+        rl.relay(1, p)
+    cl.own(me.q, wc.at[me.q])
+    xg.first()
+    for q in others:
+        mail.send(jb.at[q], jall.at[me.q], rj.at[me.q], me.mate(q))
+    for k in range(2, last):
+        for p in pieces:
+            rl.relay(k, p)
+    xg.second()
+    for q in others:
+        here = cl.slot(me.z, q)
+        mail.arrived(here, rwc.at[q], me.partner)
+        cl.own(q, here)
+    for p in pieces:
+        rl.relay(last, p)
+    xg.last(pieces[:3])
+
+    tile = length // 4
+
+    def project_rec(q):
+        at = pl.ds(pl.multiple_of(q * tile, tile), tile)
+        product = jnp.dot(xall[at], rwall[...], preferred_element_type=f32).astype(bf16)
+        projr[at] = product
+        rext[pl.ds(pl.multiple_of(q * tile + rtop, 16), tile)] = product[:, :rwid].astype(f32)
+
+    @pl.loop(0, 3)
     def _(i):
-        base = pl.multiple_of(i * seg, 16)
-        rext[pl.ds(pl.multiple_of(base + top, 8), seg)] = proj[pl.ds(base, seg), pl.ds(rec_at, rwid)].astype(f32)
-
-    @pl.when(me.has_down)
-    def _():
-        mail.arrived(halo, rh.at[0], me.partner)
-        rext[pl.ds(0, top)] = halo[:, pl.ds(rec_at, rwid)].astype(f32)
+        project_rec((me.q // 2 + i // 2) % 2 * 2 + (me.q % 2 + i % 2) % 2)
+
+    for n, p in enumerate(pieces):
+        cl.relay(1, p, n < 2, True)
+    xg.third()
+    xg.last(pieces[3:])
+    project_rec(me.qd)
+
+    mail.send(rext.at[pl.ds(length, rtop)], rext.at[pl.ds(0, rtop)], rh.at[0], me.up, me.has_up)
+    for p in pieces[2:]:
+        cl.relay(1, p, True, False)
+    for k in range(2, last):
+        for n, p in enumerate(pieces):
+            cl.relay(k, p, n < 1, True)
 
     @pl.when(jnp.logical_not(me.has_down))
     def _():
-        rext[pl.ds(0, top)] = jnp.zeros((top, rwid), f32)
+        rext[pl.ds(0, rtop)] = jnp.zeros((rtop, rwid), f32)
+        gext[pl.ds(0, top)] = jnp.zeros((top, cw), f32)
+
+    for q in others:
+        mail.arrived(jall.at[q], rj.at[q], me.partner)
 
     softened = rpar[me.q, pl.ds(s_lags + 1, 1), :]
 
     @pl.loop(0, SEGMENTS)
-    def _(i):
+    def _(n):
+        i = SEGMENTS - 1 - n
+
+        @pl.when(jnp.logical_and(i == 0, me.has_down))
+        def _():
+            mail.arrived(rext.at[pl.ds(0, rtop)], rh.at[0], me.partner)
+
         base = pl.multiple_of(i * seg, 8)
-        window = rext[pl.ds(pl.multiple_of(base + top - 8, 8), seg + 8)]
+        window = rext[pl.ds(pl.multiple_of(base + rtop - 8, 8), seg + 8)]
         smooth = jnp.zeros((seg, rwid), f32)
         for k in range(s_lags + 1):
             smooth = smooth + rpar[me.q, pl.ds(k, 1), :] * window[8 - s_lags + k : 8 - s_lags + k + seg]
         smooth = smooth.astype(bf16)
         gates = jax.nn.sigmoid(jnp.dot(smooth, maps[...], preferred_element_type=f32))
         retain, admit = gates[:, :rwid], gates[:, fold * 128 : fold * 128 + rwid]
-        wide = jump[pl.ds(base, seg)]
-        moved = wide[:, :rwid]
-        for lead in {q * rwid % 128 for q in range(4)} - {0}:
-            moved = jnp.where(me.q * rwid % 128 == lead, wide[:, lead : lead + rwid], moved)
+        wide = jall[i // 2].astype(f32)
+        moved = jnp.where(i % 2 == 0, wide[:, :rwid], wide[:, rwid:])
         log_decay = moved - retain * softened
         decay = jnp.exp(log_decay)
         inflow = jnp.sqrt(minus_expm1(2.0 * log_decay)) * admit * smooth.astype(f32)
@@ -518,36 +502,17 @@
             product, state = product * p, p * state + s
         carry[pl.ds(2 * f, 1)] = product
         carry[pl.ds(2 * f + 1, 1)] = state
-    for device in lined:
-        mail.send(carry, cr_all.at[me.z], rc.at[me.z], device)
-
-    @pl.loop(0, SEGMENTS)
-    def _(i):
-        base = pl.multiple_of(i * seg, 16)
-        gext[pl.ds(pl.multiple_of(base + top, 8), seg)] = columns(proj, base, seg)
-
-    @pl.when(me.has_down)
-    def _():
-        gext[pl.ds(0, top)] = columns(halo, 0, top)
-
-    @pl.when(jnp.logical_not(me.has_down))
-    def _():
-        gext[pl.ds(0, top)] = jnp.zeros((top, cw), f32)
-
-    def line_step(k):
-        for origin, there, on, more in (
-            (me.z - k, me.z >= k, me.up, me.has_up),
-            (me.z + k, me.z + k < planes, me.down, me.has_down),
-        ):
-            pl.when(there)(functools.partial(mail.arrived, wz.at[origin], rz.at[origin], me.partner))
-            if k < planes - 1:
-                mail.send(wz.at[origin], wz.at[origin], rz.at[origin], on, jnp.logical_and(there, more))
-            hand_over(wz.at[origin], origin, there)
-
     for k in range(1, planes):
-        z = (me.z + k) % planes
-        mail.arrived(cr_all.at[z], rc.at[z], me.partner)
-    cr_all[me.z] = carry[...]
+        mail.send(carry, cr_all.at[me.z], rc.at[me.z], lined[k - 1], me.z + k < planes)
+    for k in range(2, last):
+        for p in pieces[1:]:
+            cl.relay(k, p, True, False)
+    for p in parts[1:]:
+        out_own(p)
+
+    for k in range(1, planes):
+        z = me.z - k
+        pl.when(z >= 0)(functools.partial(mail.arrived, cr_all.at[z], rc.at[z], me.partner))
     entering = []
     for f in range(fold):
         held = jnp.zeros((1, 128), f32)
@@ -559,27 +524,46 @@
             held = ends[2 * f][i : i + 1] * held + ends[2 * f + 1][i : i + 1]
     own_at = pl.multiple_of(mine * width, 128)
     for i in range(SEGMENTS):
-        rows = pl.ds(i * seg, seg)
-        state = [dec[f, rows] * entering[f * SEGMENTS + i] + inf[f, rows] for f in range(fold)]
+        here = pl.ds(i * seg, seg)
+        state = [dec[f, here] * entering[f * SEGMENTS + i] + inf[f, here] for f in range(fold)]
         state = jnp.concatenate(state, axis=1)[:, :rwid]
-        result = gelu(proj[rows, pl.ds(gate_at, rwid)].astype(f32)) * state
+        result = gelu(projr[here, pl.ds(rwid, rwid)].astype(f32)) * state
         fill = jnp.zeros((seg, width - cw - rwid), f32)
-        yall[rows, pl.ds(pl.multiple_of(own_at + cw, 128), width - cw)] = jnp.concatenate([result, fill], axis=1).astype(bf16)
-
-    half_rows = length // 2
+        yall[here, pl.ds(pl.multiple_of(own_at + cw, 128), width - cw)] = jnp.concatenate([result, fill], axis=1).astype(bf16)
+
+    half_length = length // 2
 
     def gather(lane, lanes, recv, recv_pair):
         def slot(q, c, h):
             spot = pl.ds(pl.multiple_of((q * 2 + c) * width + lane, 128), lanes)
-            return yall.at[pl.ds(h * half_rows, half_rows), spot]
+            return yall.at[pl.ds(h * half_length, half_length), spot]
 
         return PlaneGather(me, mail, lambda h: slot(me.q, me.c, h), slot, recv, recv_pair)
 
     vg = gather(cw, width - cw, rv, rq)
     vg.start()
-
-    @pl.loop(0, length // 64)
+    for p in pieces:
+        cl.relay(last, p)
+
+    @pl.loop(0, 4)
     def _(i):
+        at = pl.ds(pl.multiple_of(i * tile, tile), tile)
+        product = jnp.dot(xall[at], cwall[...], preferred_element_type=f32).astype(bf16).astype(f32)
+        glu = (product[:, :cw] * jax.nn.sigmoid(product[:, cw:])).astype(bf16).astype(f32)
+        gext[pl.ds(pl.multiple_of(i * tile + top, 8), tile)] = glu
+
+    mail.send(gext.at[pl.ds(length, top)], gext.at[pl.ds(0, top)], rh.at[1], me.up, me.has_up)
+    for p in parts:
+        ol.relay(1, p)
+    strips = length // 64
+
+    def filter_strip(n):
+        i = strips - 1 - n
+
+        @pl.when(jnp.logical_and(i == 0, me.has_down))
+        def _():
+            mail.arrived(gext.at[pl.ds(0, top)], rh.at[1], me.partner)
+
         base = pl.multiple_of(i * 64, 8)
         window = gext[pl.ds(base, 64 + top)]
         total = jnp.zeros((64, cw), f32) + cpar[pl.ds(c_lags + 1, 1), :]
@@ -593,12 +577,15 @@
         spread = jnp.sum(off * off, axis=1, keepdims=True)
         stat[pl.ds(base, 64)] = jnp.where(lane == 0, part_sum, spread)
 
+    pl.loop(0, strips // 4)(filter_strip)
+    vg.first()
+    pl.loop(strips // 4, strips)(filter_strip)
+
     packed = stat[...].T
     st_all[mine] = packed[0:8]
     for device in mates:
         mail.send(st_all.at[mine], st_all.at[mine], rs.at[mine], device)
 
-    line_step(1)
     for k in range(1, 8):
         d = (mine + k) % 8
         mail.arrived(st_all.at[d], rs.at[d], me.partner)
@@ -614,42 +601,38 @@
 
     @pl.loop(0, SEGMENTS)
     def _(i):
-        rows = pl.ds(pl.multiple_of(i * seg, 16), seg)
-        pair = stat[rows]
-        v = (filt[rows] - pair[:, 0:1]) * pair[:, 1:2] * cpar[pl.ds(c_lags + 2, 1), :]
-        yall[rows, pl.ds(own_at, cw)] = (v * jax.nn.sigmoid(v)).astype(bf16)
+        here = pl.ds(pl.multiple_of(i * seg, 16), seg)
+        pair = stat[here]
+        v = (filt[here] - pair[:, 0:1]) * pair[:, 1:2] * cpar[pl.ds(c_lags + 2, 1), :]
+        yall[here, pl.ds(own_at, cw)] = (v * jax.nn.sigmoid(v)).astype(bf16)
 
     yg = gather(0, cw, ry, rp)
     yg.start()
-    vg.first()
+    vg.second()
     yg.first()
-    for k in range(2, planes - 1):
-        line_step(k)
-    vg.second()
+    for k in range(2, last):
+        for p in parts:
+            ol.relay(k, p)
+    vg.third()
     yg.second()
-    vg.third()
     yg.third()
-    line_step(planes - 1)
-    for k in range(part):
-        mail.arrived(wp.at[k], rw.at[k], me.partner)
-    vg.last()
-    yg.last()
-    mail.finish()
+    vg.last(pieces)
+    yg.last(pieces)
 
     used, cols = cw + rwid, w_ref.shape[1]
-    tile = length // 8
-
-    def multiply(d):
-        rows = pl.ds(pl.multiple_of(d * tile, 16), tile)
-        for k in range(part):
-            total = jnp.zeros((tile, cols), f32)
-            for q in range(4):
-                for c, block in ((me.c, wz.at[me.c * part + k]), (1 - me.c, wp.at[k])):
-                    left = yall[rows, pl.ds(pl.multiple_of((q * 2 + c) * width, 128), width)]
-                    total = total + jnp.dot(
-                        left[:, :used], block[pl.ds(q * used, used)], preferred_element_type=f32
-                    )
-            cbuf[d, k] = total.astype(bf16)
+    tile_rows = length // 8
+    upward = me.z < part
+
+    def multiply(d, k):
+        here = pl.ds(pl.multiple_of(d * tile_rows, 16), tile_rows)
+        total = jnp.zeros((tile_rows, cols), f32)
+        for q in range(4):
+            for c, block in ((me.c, wz.at[me.c * part + k]), (1 - me.c, wp.at[k])):
+                left = yall[here, pl.ds(pl.multiple_of((q * 2 + c) * width, 128), width)]
+                total = total + jnp.dot(
+                    left[:, :used], block[pl.ds(q * used, used)], preferred_element_type=f32
+                )
+        cbuf[d, k] = total.astype(bf16)
 
     def place(q, c, k):
         return out.at[:, pl.ds(pl.multiple_of(((c * part + k) * 4 + q) * cols, 128), cols)]
@@ -666,17 +649,29 @@
             recv_sem=lr.at[mine, k], device_id=me.at(me.z * 4 + q, c), device_id_type=MESH,
         )
 
-    @pl.loop(0, 7)
-    def _(i):
-        q, c = target(i)
-        multiply(q * 2 + c)
-        for k in range(part):
+    def kept(k):
+        return pltpu.make_async_copy(cbuf.at[mine, k], place(me.q, me.c, k), ls.at[7, k])
+
+    def round_of(n):
+        k = jnp.where(upward, n, part - 1 - n)
+
+        @pl.loop(0, 7)
+        def _(i):
+            q, c = target(i)
+            multiply(q * 2 + c, k)
             parcel(i, k).start()
 
-    multiply(mine)
-    kept = [pltpu.make_async_copy(cbuf.at[mine, k], place(me.q, me.c, k), ls.at[7, k]) for k in range(part)]
-    for copy in kept:
-        copy.start()
+        multiply(mine, k)
+        kept(k).start()
+
+    for n in range(part):
+        k = jnp.where(upward, n, part - 1 - n)
+        if n == part - 1:
+            for p in parts:
+                ol.relay(last, p)
+        for p in parts:
+            mail.arrived(wp.at[k, pl.ds(p * tall, tall)], rw.at[k, p], me.partner)
+        round_of(n)
 
     @pl.loop(0, 7)
     def _(i):
@@ -685,32 +680,42 @@
             mail.arrived(place(q, c, k), lr.at[q * 2 + c, k], me.partner)
             parcel(i, k).wait_send()
 
-    for copy in kept:
-        copy.wait()
-
-
-def core(planes, proj, jump, cpar, rpar, dmap, imap, weights, lags, cw):
-    length, rwid = jump.shape[0], rpar.shape[2]
+    for k in range(part):
+        kept(k).wait()
+    mail.finish()
+
+
+def layer(planes, tokens, gain, wr, wc, jb, cpar, rpar, dmap, imap, weights, lags):
+    rows, width_in = tokens.shape
+    length = 8 * rows
+    cw, rwid = wc.shape[2] // 2, rpar.shape[2]
+    depth = wr.shape[1]
     used, cols = cw + rwid, weights.shape[1]
     width = used + -used % 128
     fold = (rwid + 127) // 128
     f32, bf16 = jnp.float32, jnp.bfloat16
     dma, vmem = pltpu.SemaphoreType.DMA, pltpu.VMEM
     top = lags[0] + -lags[0] % 16
+    rtop = lags[1] + -lags[1] % 16
     part = planes // 2
+    deep = planes * 4 * depth
     return pl.pallas_call(
-        functools.partial(core_kernel, planes, lags),
-        out_shape=jax.ShapeDtypeStruct((length // 8, planes * 4 * cols), bf16),
-        in_specs=[VMEM] * 7,
+        functools.partial(layer_kernel, planes, lags),
+        out_shape=jax.ShapeDtypeStruct((rows, planes * 4 * cols), bf16),
+        in_specs=[VMEM] * 10,
         out_specs=ANY,
         scratch_shapes=[
+            vmem((length, width_in), bf16),
+            vmem((deep, wr.shape[2]), bf16),
+            vmem((deep, wc.shape[2]), bf16),
+            vmem((length, wr.shape[2]), bf16),
+            vmem(jb.shape, bf16),
             vmem((planes,) + weights.shape, bf16),
             vmem((part,) + weights.shape, bf16),
             vmem((length, 8 * width), bf16),
-            vmem((8, part, length // 8, cols), bf16),
-            vmem((top, proj.shape[1]), bf16),
+            vmem((8, part, rows, cols), bf16),
             vmem((top + length, cw), f32),
-            vmem((top + length, rwid), f32),
+            vmem((rtop + length, rwid), f32),
             vmem((length, cw), f32),
             vmem((fold, length, 128), f32),
             vmem((fold, length, 128), f32),
@@ -719,13 +724,15 @@
             vmem((8, 8, length), f32),
             vmem((8, 128), f32),
             vmem((planes, 8, 128), f32),
-            dma((64 + 8 * planes,)), dma((4, 2)), dma((4, 2)), dma((4, 2)), dma((4, 2)), dma((planes,)), dma((part,)),
-            dma((1,)), dma((8,)), dma((planes,)), dma((8, part)), dma((8, part)),
+            dma((100 + 20 * planes,)), dma((4, 2)), dma((4, 2)), dma((4,)), dma((4,)),
+            dma((planes, 4)), dma((planes, 4)), dma((planes, OUT_PARTS)), dma((4,)),
+            dma((4, 2)), dma((4, 2)), dma((4, 2)), dma((4, 2)), dma((part, OUT_PARTS)),
+            dma((2,)), dma((8,)), dma((planes,)), dma((8, part)), dma((8, part)),
         ],
         compiler_params=pltpu.CompilerParams(
-            collective_id=2, has_side_effects=True, vmem_limit_bytes=60 * 1024 * 1024
+            collective_id=0, has_side_effects=True, vmem_limit_bytes=60 * 1024 * 1024
         ),
-    )(proj, jump, cpar, rpar, dmap, imap, weights)
+    )(tokens, gain, wr, wc, jb, cpar, rpar, dmap, imap, weights)
 
 
 def plane_shards(
@@ -758,10 +765,11 @@
         size = a.shape[axis] // 4
         return lax.dynamic_slice_in_dim(a, q * size, size, axis)
 
-    pieces = jnp.concatenate([by_mate(w) for w in (conv_val_w, conv_gate_w, rec_gate_w, rec_in_w)], axis=2)
-    projected, jall = enter(planes, tokens, norm_gain[None], pieces, decay_jump)
+    wr = jnp.concatenate([by_mate(w) for w in (rec_in_w, rec_gate_w)], axis=2)
+    wc = jnp.concatenate([by_mate(w) for w in (conv_val_w, conv_gate_w)], axis=2)
+    half = decay_jump.shape[0] // 2
     cw, rw = conv_val_w.shape[1] // 4, rec_in_w.shape[1] // 4
-    jump = jall.reshape(-1, jall.shape[2])
+    jb = decay_jump.astype(jnp.bfloat16).reshape(2, half, 4, rw).transpose(2, 1, 0, 3).reshape(4, half, 2 * rw)
     cols = out_conv_w.shape[1]
     rows_by_mate = jnp.concatenate(
         [out_conv_w.reshape(4, cw, cols), out_rec_w.reshape(4, rw, cols)], axis=1
@@ -769,7 +777,9 @@
     cpar = mine(jnp.concatenate([conv_taps.astype(f32), conv_bias[None], conv_gain[None]]), 1)
     rpar = by_mate(jnp.concatenate([short_taps.astype(f32), RATE_SCALE * jax.nn.softplus(-decay_base)[None]]))
     lags = (conv_taps.shape[0] - 1, short_taps.shape[0] - 1)
-    return core(planes, projected, jump, cpar, rpar, decay_map, input_map, rows_by_mate, lags, cw)
+    return layer(
+        planes, tokens, norm_gain[None], wr, wc, jb, cpar, rpar, decay_map, input_map, rows_by_mate, lags
+    )
 
 
 def solution(mesh):

time: 203 us -> 182 us (0.90)
  Pallas kernels: 191 us -> 166 us
  local copies, waits for them, and re-layouts: 5.99 us -> 8.69 us
    pallas_call x2 -> x1, Pallas kernels: 191 us -> 166 us  [layer(): pl.pallas_call(functools.partial(layer_kernel, planes, lags), out_shape=j...]
    reshape x0 -> x3, local copies, waits for them, and re-layouts: none -> 2.73 us  [plane_shards(): decay_jump.astype(jnp.bfloat16).reshape(2, half, 4, rw)]
    unnamed x15 -> x17, local copies, waits for them, and re-layouts: 4.37 us -> 4.34 us
where the time goes in v1:
time: 182 us
  Pallas kernels  166 us (91%)
  local copies, waits for them, and re-layouts  8.69 us (5%)
  other arithmetic  6.48 us (4%)
    pallas_call x1, Pallas kernels, layer(): pl.pallas_call(functools.partial(layer_kernel, planes, lags), out_shape=j...  166 us
    unnamed x17, local copies, waits for them, and re-layouts  4.34 us

profile of v1, /device:TPU:0, one launch (start us, length us, event | category | flops | bytes accessed | tf_op | source)
XLA Modules:
  0.0 181.5 jit_solution(15123804878900675326)
XLA Ops:
  0.0 0.0 copy-start.5
  0.0 0.7 fusion.2
  0.7 0.1 concatenate.27
  0.8 0.8 reshape.42
  1.6 0.6 maximum_bitcast_fusion.rpar
  2.2 0.8 convert_element_type.8
  3.0 1.3 fusion.1.cpar
  4.4 0.0 copy-start.1
  4.4 1.1 copy.22
  5.5 0.2 copy.23
  5.7 0.0 copy-done.5
  5.7 0.1 copy.24
  5.8 0.0 copy-start.2
  5.8 0.2 copy.25
  6.0 0.9 pad_maximum_fusion.2.wc
  6.9 0.0 copy-done.1
  6.9 0.2 copy.20
  7.1 0.2 copy.21
  7.3 0.0 copy-done.2
  7.3 0.2 copy.18
  7.4 0.0 copy-start
  7.5 0.2 copy.19
  7.7 1.2 pad_maximum_fusion.wr
  8.9 0.0 copy-done
  8.9 0.1 convert_element_type.7
  8.9 0.7 reshape.37
  9.6 0.0 copy-start.3
  9.6 0.0 copy-start.4
  9.6 0.8 copy.29
  10.4 1.3 reshape.38.jb
  11.7 0.0 copy-done.3
  11.7 0.0 copy-done.4
  11.7 0.9 pad_maximum_fusion.1
  12.6 166.2 %shard_map.154 = bf16[192,4096]{1,0:T(8,128)(2,1)} custom-call(bf16[192,4096]{1,0:T(8,128)(2,1)} %x_ref.1, f32[1,4096]{1,0:T(1,128)} %bitcast.31, bf16[4,256,384]{2,1,0:T(8,128)(2,1)} %pad_maximum_fusion.wr, bf16[4,256,256]{2,1,0:T(8,128)(2,1)} %pad_maximum_fusion.2.wc, bf16[4,192,384]{2,1,0:T(8,128)(2,1)} %reshape.38.jb, f32[33,128]{1,0:T(8,128)} %fusion.1.cpar, ...), custom_call_target="tpu_custom_call" | custom-call | tf_op jit(solution)/shard_map/pallas_call | solution.py:702
  178.8 2.7 %copy.31 = bf16[192,4096]{1,0:T(8,128)(2,1)} copy(bf16[192,4096]{1,0:T(8,128)(2,1)} %shard_map.154) | data formatting | bytes 3145728
  (1 shorter events, 0.0 us)
Async XLA Ops:
  0.0 5.7 %copy-start.5 = (bf16[256,512]{1,0:T(8,128)(2,1)S(1)}, bf16[256,512]{1,0:T(8,128)(2,1)}, u32[]{:S(2)}) copy-start(bf16[256,512]{1,0:T(8,128)(2,1)} %param.19) | copy-start | bytes 786436
  4.4 2.5 %copy-start.1 = (bf16[256,768]{1,0:T(8,128)(2,1)S(1)}, bf16[256,768]{1,0:T(8,128)(2,1)}, u32[]{:S(2)}) copy-start(bf16[256,768]{1,0:T(8,128)(2,1)} %param.20) | copy-start | bytes 1179652
  5.8 1.4 copy-start.2
  7.4 1.4 copy-start
  9.6 2.1 %copy-start.3 = (bf16[768,256]{1,0:T(8,128)(2,1)S(1)}, bf16[768,256]{1,0:T(8,128)(2,1)}, u32[]{:S(2)}) copy-start(bf16[768,256]{1,0:T(8,128)(2,1)} %param.31) | copy-start | bytes 1179652
  9.6 2.1 %copy-start.4 = (bf16[512,256]{1,0:T(8,128)(2,1)S(1)}, bf16[512,256]{1,0:T(8,128)(2,1)}, u32[]{:S(2)}) copy-start(bf16[512,256]{1,0:T(8,128)(2,1)} %param.30) | copy-start | bytes 786436

commit v2 on v1

--- a/solution.py
+++ b/solution.py
@@ -223,47 +223,51 @@
 
 
 class PlaneGather:
-    def __init__(self, me, mail, own, slot, recv, recv_pair):
-        self.me, self.mail, self.own, self.slot = me, mail, own, slot
+    def __init__(self, me, mail, slot, recv, recv_pair):
+        self.me, self.mail, self.slot = me, mail, slot
         self.recv, self.recv_pair = recv, recv_pair
+        self.parts = recv.shape[1]
+        self.half = self.parts // 2
 
     def start(self):
         me, mail = self.me, self.mail
-        for h in (0, 1):
-            for q, half in ((me.qx, h), (me.qy, 1 - h)):
-                mail.send(self.own(half), self.slot(me.q, me.c, half), self.recv.at[me.q, half], me.mate(q))
-        for half in (0, 1):
-            mail.send(self.own(half), self.slot(me.q, me.c, half), self.recv_pair.at[me.q, half], me.partner)
-
-    def took(self, q, half):
-        me, mail = self.me, self.mail
-        here = self.slot(q, me.c, half)
-        mail.arrived(here, self.recv.at[q, half], me.partner)
+        for h in range(self.parts):
+            for q, part in ((me.qx, h), (me.qy, (h + self.half) % self.parts)):
+                own = self.slot(me.q, me.c, part)
+                mail.send(own, own, self.recv.at[me.q, part], me.mate(q))
+        for part in range(self.parts):
+            self.share(me.q, part, self.slot(me.q, me.c, part))
+
+    def took(self, q, part):
+        here = self.slot(q, self.me.c, part)
+        self.mail.arrived(here, self.recv.at[q, part], self.me.partner)
         return here
 
-    def share(self, q, half, here):
-        self.mail.send(here, here, self.recv_pair.at[q, half], self.me.partner)
-
-    def first(self):
+    def share(self, q, part, here):
+        self.mail.send(here, here, self.recv_pair.at[q, part], self.me.partner)
+
+    def first(self, i):
         me = self.me
-        for q, half, to in ((me.qx, 0, me.qy), (me.qy, 1, me.qx)):
-            here = self.took(q, half)
-            self.mail.send(here, here, self.recv.at[q, half], me.mate(to))
-            self.share(q, half, here)
+        for q, part, to in ((me.qx, i, me.qy), (me.qy, self.half + i, me.qx)):
+            here = self.took(q, part)
+            self.mail.send(here, here, self.recv.at[q, part], me.mate(to))
+            self.share(q, part, here)
 
     def second(self):
-        for q, half in ((self.me.qx, 1), (self.me.qy, 0)):
-            self.share(q, half, self.took(q, half))
+        for i in range(self.half):
+            for q, part in ((self.me.qx, self.half + i), (self.me.qy, i)):
+                self.share(q, part, self.took(q, part))
 
     def third(self):
-        for half in (0, 1):
-            self.share(self.me.qd, half, self.took(self.me.qd, half))
+        for i in range(self.half):
+            for part in (i, self.half + i):
+                self.share(self.me.qd, part, self.took(self.me.qd, part))
 
     def last(self, origins):
         me = self.me
         for q in origins:
-            for half in (0, 1):
-                self.mail.arrived(self.slot(q, 1 - me.c, half), self.recv_pair.at[q, half], me.partner)
+            for part in range(self.parts):
+                self.mail.arrived(self.slot(q, 1 - me.c, part), self.recv_pair.at[q, part], me.partner)
 
 
 def minus_expm1(y):
@@ -288,27 +292,48 @@
             if wanted:
                 self.mail.send(src, self.slot(me.z, piece), self.recv.at[me.z, piece], device, has)
 
+    def ways(self, k):
+        me = self.me
+        return (
+            (me.z - k, me.z >= k, me.up, me.has_up),
+            (me.z + k, me.z + k < self.planes, me.down, me.has_down),
+        )
+
+    def take(self, origin, piece, when):
+        here, sem = self.slot(origin, piece), self.recv.at[origin, piece]
+        pl.when(when)(functools.partial(self.mail.arrived, here, sem, self.me.partner))
+        if self.seen is not None:
+            self.seen(origin, piece, when)
+        return here, sem
+
     def relay(self, k, piece, up=True, down=True):
-        me = self.me
-        for wanted, origin, there, on, more in (
-            (up, me.z - k, me.z >= k, me.up, me.has_up),
-            (down, me.z + k, me.z + k < self.planes, me.down, me.has_down),
-        ):
+        for wanted, (origin, there, on, more) in zip((up, down), self.ways(k)):
             if wanted:
-                here, sem = self.slot(origin, piece), self.recv.at[origin, piece]
-                pl.when(there)(functools.partial(self.mail.arrived, here, sem, me.partner))
-                if k < self.planes - 1:
-                    self.mail.send(here, here, sem, on, jnp.logical_and(there, more))
-                if self.seen is not None:
-                    self.seen(origin, piece, there)
+                when = jnp.logical_and(there, more)
+                here, sem = self.take(origin, piece, when)
+                self.mail.send(here, here, sem, on, when)
+
+    def settle(self, k, piece):
+        for origin, there, _, more in self.ways(k):
+            self.take(origin, piece, jnp.logical_and(there, jnp.logical_not(more)))
+
+
+def small_softplus(v):
+    u = jnp.exp(-jnp.abs(v))
+    series = jnp.zeros_like(u)
+    for n in (8.0, 7.0, 6.0, 5.0, 4.0, 3.0, 2.0, 1.0):
+        series = 1.0 / n - u * series
+    return jnp.maximum(v, 0.0) + jnp.where(u < 0.1, u * series, jnp.log(1.0 + u))
 
 
 OUT_PARTS = 4
 
 
 def layer_kernel(
-    planes, lags, x_ref, gain, wr, wc, jb, cpar, rpar, dmap, imap, w_ref,
-    out, xall, rwall, cwall, projr, jall, wz, wp, yall, cbuf, gext, rext, filt, dec, inf, maps, stat,
+    planes, lags, tokens, gain_in, val_w, gate_w, rgate_w, rin_w, taps_in, bias_in, cgain_in, staps_in,
+    dmap_in, imap_in, base_in, jump_in, ocw, orw,
+    out, x_ref, gain, rin_s, rgate_s, wr, wc, taps, bias, cgain, staps, dmap, imap, rbase, jump, jb, cpar, rpar,
+    ld, xall, rwall, cwall, projr, jall, wz, wp, yall, cbuf, gext, rext, filt, dec, inf, maps, stat,
     st_all, carry, cr_all,
     send, rx, rpx, rwr, rwc, zr, zc, zo, rj, ry, rp, rv, rq, rw, rh, rs, rc, ls, lr,
 ):
@@ -318,7 +343,7 @@
     f32, bf16 = jnp.float32, jnp.bfloat16
     rows, depth = x_ref.shape[0], wr.shape[1]
     length = xall.shape[0]
-    cw, rwid = gext.shape[1], rpar.shape[2]
+    cw, rwid = gext.shape[1], rpar.shape[1]
     seg = length // SEGMENTS
     top = gext.shape[0] - length
     rtop = rext.shape[0] - length
@@ -329,11 +354,43 @@
     others = (me.qx, me.qy, me.qd)
     pieces = (me.q,) + others
     parts = tuple(range(OUT_PARTS))
-    tall = w_ref.shape[0] // OUT_PARTS
+    tall = wz.shape[1] // OUT_PARTS
     last = planes - 1
     mates = [me.at(me.z * 4 + (me.q + dq) % 4, c) for dq in range(4) for c in (me.c, 1 - me.c)][1:]
     lined = [me.at((me.s + 4 * k) % (4 * planes), me.c) for k in range(1, planes)]
+    loads = []
+
+    def load(src, dst):
+        copy = pltpu.make_async_copy(src, dst, ld.at[len(loads)])
+        loads.append(copy)
+        copy.start()
+        return copy
+
+    got_rec = [load(rin_w, rin_s), load(rgate_w, rgate_s)]
+    got_x = [load(tokens, x_ref), load(gain_in, gain)]
+    got_conv = []
+    for q in range(4):
+        got_conv.append(load(val_w.at[:, pl.ds(q * cw, cw)], wc.at[q, :, pl.ds(0, cw)]))
+        got_conv.append(load(gate_w.at[:, pl.ds(q * cw, cw)], wc.at[q, :, pl.ds(cw, cw)]))
+    got_out = []
+    for q in range(4):
+        at = q * (cw + rwid)
+        got_out.append(load(ocw.at[pl.ds(q * cw, cw)], wz.at[me.z, pl.ds(at, cw)]))
+        got_out.append(load(orw.at[pl.ds(q * rwid, rwid)], wz.at[me.z, pl.ds(at + cw, rwid)]))
+    got_jump = [load(jump_in, jump)]
+    got_small = [
+        load(src, dst)
+        for src, dst in (
+            (taps_in, taps), (bias_in, bias), (cgain_in, cgain), (staps_in, staps),
+            (dmap_in, dmap), (imap_in, imap), (base_in, rbase),
+        )
+    ]
     greet(me, mates + lined, False)
+    for copy in got_rec:
+        copy.wait()
+    for q in range(4):
+        lanes = slice(q * rwid, (q + 1) * rwid)
+        wr[q] = jnp.concatenate([rin_s[:, lanes], rgate_s[:, lanes]], axis=1)
 
     def of_rows(ref):
         def slot(origin, piece):
@@ -352,12 +409,14 @@
     ol = Line(me, mail, planes, lambda origin, p: wz.at[origin, pl.ds(p * tall, tall)], zo, theirs_too)
 
     def out_own(p):
-        ol.own(p, w_ref.at[pl.ds(p * tall, tall)])
+        ol.own(p, wz.at[me.z, pl.ds(p * tall, tall)])
 
     for q in others:
         mail.send(wr.at[q], rl.slot(me.z, me.q), rwr.at[me.q], me.mate(q))
     rl.own(me.q, wr.at[me.q])
 
+    for copy in got_x:
+        copy.wait()
     first_row = mine * rows
 
     @pl.loop(0, rows // 16)
@@ -367,29 +426,47 @@
         place = pl.ds(pl.multiple_of(first_row + i * 16, 16), 16)
         xall[place] = (values * inverse * gain[...]).astype(bf16)
 
-    half_rows = rows // 2
+    part_rows = rows // rx.shape[1]
 
     def xslot(q, c, h):
-        return xall.at[pl.ds(pl.multiple_of((q * 2 + c) * rows + h * half_rows, 16), half_rows)]
-
-    xg = PlaneGather(me, mail, lambda h: xslot(me.q, me.c, h), xslot, rx, rpx)
+        return xall.at[pl.ds(pl.multiple_of((q * 2 + c) * rows + h * part_rows, 16), part_rows)]
+
+    xg = PlaneGather(me, mail, xslot, rx, rpx)
     xg.start()
+    for copy in got_conv + got_out:
+        copy.wait()
     for q in others:
         mail.send(wc.at[q], cl.slot(me.z, me.q), rwc.at[me.q], me.mate(q))
     out_own(0)
-    kept_here = [
-        mail.local(wr.at[me.q], rl.slot(me.z, me.q)),
-        mail.local(wc.at[me.q], cl.slot(me.z, me.q)),
-        mail.local(w_ref, wz.at[me.z]),
-        mail.local(jb.at[me.q], jall.at[me.q]),
-    ]
+    out_own(1)
+    kept_here = [mail.local(wr.at[me.q], rl.slot(me.z, me.q)), mail.local(wc.at[me.q], cl.slot(me.z, me.q))]
     for entry in kept_here:
         mail.open.remove(entry)
         entry[0]()
     for p in parts:
-        rest = pl.ds(p * tall, tall)
-        place = me.z - (1 - me.c) * part
-        mail.send(w_ref.at[rest], wp.at[place, rest], rw.at[place, p], me.partner, me.z // part != me.c)
+        theirs_too(me.z, p, True)
+    for copy in got_jump + got_small:
+        copy.wait()
+    half = jump.shape[0] // 2
+    for q in range(4):
+        lanes = slice(q * rwid, (q + 1) * rwid)
+        jb[q] = jnp.concatenate([jump[:half, lanes], jump[half:, lanes]], axis=1).astype(bf16)
+    jall[me.q] = jb[me.q]
+    own_lanes = pl.ds(pl.multiple_of(me.q * cw, 128), cw)
+    cpar[pl.ds(0, c_lags + 1)] = taps[:, own_lanes].astype(f32)
+    cpar[pl.ds(c_lags + 1, 1)] = bias[:, own_lanes]
+    cpar[pl.ds(c_lags + 2, 1)] = cgain[:, own_lanes]
+    window = -(-rwid // 128) * 128
+    wide_lanes = pl.ds(pl.multiple_of(me.q * rwid // 128 * 128, 128), window)
+
+    def own_rec(values):
+        moved = values[:, :rwid]
+        for lead in sorted({q * rwid % 128 for q in range(4)} - {0}):
+            moved = jnp.where(me.q * rwid % 128 == lead, values[:, lead : lead + rwid], moved)
+        return moved
+
+    rpar[pl.ds(0, s_lags + 1)] = own_rec(staps[:, wide_lanes].astype(f32))
+    rpar[pl.ds(s_lags + 1, 1)] = own_rec(RATE_SCALE * small_softplus(-rbase[:, wide_lanes]))
 
     maps[...] = jnp.zeros_like(maps)
     size = dmap.shape[1]
@@ -406,7 +483,8 @@
     for p in pieces:
         rl.relay(1, p)
     cl.own(me.q, wc.at[me.q])
-    xg.first()
+    for i in range(xg.half):
+        xg.first(i)
     for q in others:
         mail.send(jb.at[q], jall.at[me.q], rj.at[me.q], me.mate(q))
     for k in range(2, last):
@@ -417,8 +495,9 @@
         here = cl.slot(me.z, q)
         mail.arrived(here, rwc.at[q], me.partner)
         cl.own(q, here)
-    for p in pieces:
-        rl.relay(last, p)
+    for k in range(1, planes):
+        for p in pieces:
+            rl.settle(k, p)
     xg.last(pieces[:3])
 
     tile = length // 4
@@ -451,10 +530,7 @@
         rext[pl.ds(0, rtop)] = jnp.zeros((rtop, rwid), f32)
         gext[pl.ds(0, top)] = jnp.zeros((top, cw), f32)
 
-    for q in others:
-        mail.arrived(jall.at[q], rj.at[q], me.partner)
-
-    softened = rpar[me.q, pl.ds(s_lags + 1, 1), :]
+    softened = rpar[pl.ds(s_lags + 1, 1), :]
 
     @pl.loop(0, SEGMENTS)
     def _(n):
@@ -463,12 +539,16 @@
         @pl.when(jnp.logical_and(i == 0, me.has_down))
         def _():
             mail.arrived(rext.at[pl.ds(0, rtop)], rh.at[0], me.partner)
+
+        @pl.when(jnp.logical_and(i % 2 == 1, i // 2 != me.q))
+        def _():
+            mail.arrived(jall.at[i // 2], rj.at[i // 2], me.partner)
 
         base = pl.multiple_of(i * seg, 8)
         window = rext[pl.ds(pl.multiple_of(base + rtop - 8, 8), seg + 8)]
         smooth = jnp.zeros((seg, rwid), f32)
         for k in range(s_lags + 1):
-            smooth = smooth + rpar[me.q, pl.ds(k, 1), :] * window[8 - s_lags + k : 8 - s_lags + k + seg]
+            smooth = smooth + rpar[pl.ds(k, 1), :] * window[8 - s_lags + k : 8 - s_lags + k + seg]
         smooth = smooth.astype(bf16)
         gates = jax.nn.sigmoid(jnp.dot(smooth, maps[...], preferred_element_type=f32))
         retain, admit = gates[:, :rwid], gates[:, fold * 128 : fold * 128 + rwid]
@@ -507,7 +587,7 @@
     for k in range(2, last):
         for p in pieces[1:]:
             cl.relay(k, p, True, False)
-    for p in parts[1:]:
+    for p in parts[2:]:
         out_own(p)
 
     for k in range(1, planes):
@@ -531,19 +611,20 @@
         fill = jnp.zeros((seg, width - cw - rwid), f32)
         yall[here, pl.ds(pl.multiple_of(own_at + cw, 128), width - cw)] = jnp.concatenate([result, fill], axis=1).astype(bf16)
 
-    half_length = length // 2
+    part_length = length // rv.shape[1]
 
     def gather(lane, lanes, recv, recv_pair):
         def slot(q, c, h):
             spot = pl.ds(pl.multiple_of((q * 2 + c) * width + lane, 128), lanes)
-            return yall.at[pl.ds(h * half_length, half_length), spot]
-
-        return PlaneGather(me, mail, lambda h: slot(me.q, me.c, h), slot, recv, recv_pair)
+            return yall.at[pl.ds(h * part_length, part_length), spot]
+
+        return PlaneGather(me, mail, slot, recv, recv_pair)
 
     vg = gather(cw, width - cw, rv, rq)
     vg.start()
-    for p in pieces:
-        cl.relay(last, p)
+    for k in range(1, planes):
+        for p in pieces:
+            cl.settle(k, p)
 
     @pl.loop(0, 4)
     def _(i):
@@ -578,13 +659,15 @@
         stat[pl.ds(base, 64)] = jnp.where(lane == 0, part_sum, spread)
 
     pl.loop(0, strips // 4)(filter_strip)
-    vg.first()
+    vg.first(0)
     pl.loop(strips // 4, strips)(filter_strip)
 
     packed = stat[...].T
-    st_all[mine] = packed[0:8]
+    st_all[mine] = packed[0:2]
     for device in mates:
         mail.send(st_all.at[mine], st_all.at[mine], rs.at[mine], device)
+    for i in range(1, vg.half):
+        vg.first(i)
 
     for k in range(1, 8):
         d = (mine + k) % 8
@@ -609,17 +692,21 @@
     yg = gather(0, cw, ry, rp)
     yg.start()
     vg.second()
-    yg.first()
+    for i in range(yg.half):
+        yg.first(i)
     for k in range(2, last):
         for p in parts:
             ol.relay(k, p)
+    for k in range(1, last):
+        for p in parts:
+            ol.settle(k, p)
     vg.third()
     yg.second()
     yg.third()
     vg.last(pieces)
     yg.last(pieces)
 
-    used, cols = cw + rwid, w_ref.shape[1]
+    used, cols = cw + rwid, wz.shape[2]
     tile_rows = length // 8
     upward = me.z < part
 
@@ -668,7 +755,7 @@
         k = jnp.where(upward, n, part - 1 - n)
         if n == part - 1:
             for p in parts:
-                ol.relay(last, p)
+                ol.settle(last, p)
         for p in parts:
             mail.arrived(wp.at[k, pl.ds(p * tall, tall)], rw.at[k, p], me.partner)
         round_of(n)
@@ -685,54 +772,70 @@
     mail.finish()
 
 
-def layer(planes, tokens, gain, wr, wc, jb, cpar, rpar, dmap, imap, weights, lags):
+def layer(planes, lags, tokens, norm_gain, val_w, gate_w, rgate_w, rin_w, taps, bias, cgain, staps, dmap, imap, rbase, jump, ocw, orw):
     rows, width_in = tokens.shape
     length = 8 * rows
-    cw, rwid = wc.shape[2] // 2, rpar.shape[2]
-    depth = wr.shape[1]
-    used, cols = cw + rwid, weights.shape[1]
+    depth = rin_w.shape[0]
+    cw, rwid = val_w.shape[1] // 4, rin_w.shape[1] // 4
+    used, cols = cw + rwid, ocw.shape[1]
     width = used + -used % 128
     fold = (rwid + 127) // 128
     f32, bf16 = jnp.float32, jnp.bfloat16
-    dma, vmem = pltpu.SemaphoreType.DMA, pltpu.VMEM
+    dma = pltpu.SemaphoreType.DMA
     top = lags[0] + -lags[0] % 16
     rtop = lags[1] + -lags[1] % 16
     part = planes // 2
     deep = planes * 4 * depth
+
+    def vmem(*shape, dtype=bf16):
+        return pltpu.VMEM(shape, dtype)
+
+    def wide(*shape):
+        return pltpu.VMEM(shape, f32)
+
     return pl.pallas_call(
         functools.partial(layer_kernel, planes, lags),
         out_shape=jax.ShapeDtypeStruct((rows, planes * 4 * cols), bf16),
-        in_specs=[VMEM] * 10,
+        in_specs=[ANY] * 16,
         out_specs=ANY,
         scratch_shapes=[
-            vmem((length, width_in), bf16),
-            vmem((deep, wr.shape[2]), bf16),
-            vmem((deep, wc.shape[2]), bf16),
-            vmem((length, wr.shape[2]), bf16),
-            vmem(jb.shape, bf16),
-            vmem((planes,) + weights.shape, bf16),
-            vmem((part,) + weights.shape, bf16),
-            vmem((length, 8 * width), bf16),
-            vmem((8, part, rows, cols), bf16),
-            vmem((top + length, cw), f32),
-            vmem((rtop + length, rwid), f32),
-            vmem((length, cw), f32),
-            vmem((fold, length, 128), f32),
-            vmem((fold, length, 128), f32),
-            vmem((rwid, 2 * fold * 128), bf16),
-            vmem((length, 128), f32),
-            vmem((8, 8, length), f32),
-            vmem((8, 128), f32),
-            vmem((planes, 8, 128), f32),
-            dma((100 + 20 * planes,)), dma((4, 2)), dma((4, 2)), dma((4,)), dma((4,)),
+            vmem(rows, width_in), wide(1, width_in), vmem(*rin_w.shape), vmem(*rgate_w.shape),
+            vmem(4, depth, 2 * rwid), vmem(4, depth, 2 * cw),
+            vmem(*taps.shape), wide(1, 4 * cw), wide(1, 4 * cw), vmem(*staps.shape),
+            vmem(*dmap.shape), vmem(*imap.shape), wide(1, 4 * rwid), wide(*jump.shape),
+            vmem(4, jump.shape[0] // 2, 2 * rwid), wide(lags[0] + 3 + -(lags[0] + 3) % 8, cw), wide(8, rwid),
+            dma((32,)),
+            vmem(length, width_in),
+            vmem(deep, 2 * rwid),
+            vmem(deep, 2 * cw),
+            vmem(length, 2 * rwid),
+            vmem(4, jump.shape[0] // 2, 2 * rwid),
+            vmem(planes, 4 * used, cols),
+            vmem(part, 4 * used, cols),
+            vmem(length, 8 * width),
+            vmem(8, part, rows, cols),
+            wide(top + length, cw),
+            wide(rtop + length, rwid),
+            wide(length, cw),
+            wide(fold, length, 128),
+            wide(fold, length, 128),
+            vmem(rwid, 2 * fold * 128),
+            wide(length, 128),
+            wide(8, 2, length),
+            wide(8, 128),
+            wide(planes, 8, 128),
+            dma((160 + 20 * planes,)), dma((4, 4)), dma((4, 4)), dma((4,)), dma((4,)),
             dma((planes, 4)), dma((planes, 4)), dma((planes, OUT_PARTS)), dma((4,)),
-            dma((4, 2)), dma((4, 2)), dma((4, 2)), dma((4, 2)), dma((part, OUT_PARTS)),
+            dma((4, 4)), dma((4, 4)), dma((4, 4)), dma((4, 4)), dma((part, OUT_PARTS)),
             dma((2,)), dma((8,)), dma((planes,)), dma((8, part)), dma((8, part)),
         ],
         compiler_params=pltpu.CompilerParams(
             collective_id=0, has_side_effects=True, vmem_limit_bytes=60 * 1024 * 1024
         ),
-    )(tokens, gain, wr, wc, jb, cpar, rpar, dmap, imap, weights)
+    )(
+        tokens, norm_gain[None], val_w, gate_w, rgate_w, rin_w, taps, bias[None], cgain[None], staps,
+        dmap, imap, rbase[None], jump, ocw, orw,
+    )
 
 
 def plane_shards(
@@ -754,31 +857,10 @@
     out_conv_w,
     out_rec_w,
 ):
-    s = lax.axis_index("sp")
-    q = s % 4
-    f32 = jnp.float32
-
-    def by_mate(a):
-        return a.reshape(a.shape[0], 4, a.shape[1] // 4).transpose(1, 0, 2)
-
-    def mine(a, axis):
-        size = a.shape[axis] // 4
-        return lax.dynamic_slice_in_dim(a, q * size, size, axis)
-
-    wr = jnp.concatenate([by_mate(w) for w in (rec_in_w, rec_gate_w)], axis=2)
-    wc = jnp.concatenate([by_mate(w) for w in (conv_val_w, conv_gate_w)], axis=2)
-    half = decay_jump.shape[0] // 2
-    cw, rw = conv_val_w.shape[1] // 4, rec_in_w.shape[1] // 4
-    jb = decay_jump.astype(jnp.bfloat16).reshape(2, half, 4, rw).transpose(2, 1, 0, 3).reshape(4, half, 2 * rw)
-    cols = out_conv_w.shape[1]
-    rows_by_mate = jnp.concatenate(
-        [out_conv_w.reshape(4, cw, cols), out_rec_w.reshape(4, rw, cols)], axis=1
-    ).reshape(-1, cols)
-    cpar = mine(jnp.concatenate([conv_taps.astype(f32), conv_bias[None], conv_gain[None]]), 1)
-    rpar = by_mate(jnp.concatenate([short_taps.astype(f32), RATE_SCALE * jax.nn.softplus(-decay_base)[None]]))
     lags = (conv_taps.shape[0] - 1, short_taps.shape[0] - 1)
     return layer(
-        planes, tokens, norm_gain[None], wr, wc, jb, cpar, rpar, decay_map, input_map, rows_by_mate, lags
+        planes, lags, tokens, norm_gain, conv_val_w, conv_gate_w, rec_gate_w, rec_in_w, conv_taps, conv_bias,
+        conv_gain, short_taps, decay_map, input_map, decay_base, decay_jump, out_conv_w, out_rec_w,
     )
 
 

time: 182 us -> 161 us (0.88)
  Pallas kernels: 166 us -> 157 us
  other arithmetic: 6.48 us -> 0 us
  local copies, waits for them, and re-layouts: 8.69 us -> 3.97 us
    pallas_call x1, Pallas kernels: 166 us -> 157 us  [layer(): pl.pallas_call(functools.partial(layer_kernel, planes, lags), out_shape=j...]
    concatenate x4 -> x0, other arithmetic: 4.29 us -> none  [the longest x1 1.35 us: plane_shards(): jnp.concatenate([conv_taps.astype(f32), conv_bias[None], conv_gain[None]])]
    reshape x7 -> x0, local copies, waits for them, and re-layouts: 3.48 us -> none  [the longest x3 2.73 us: plane_shards(): decay_jump.astype(jnp.bfloat16).reshape(2, half, 4, rw)]
    unnamed x17 -> x1, local copies, waits for them, and re-layouts: 4.34 us -> 2.7 us
where the time goes in v2:
time: 161 us
  Pallas kernels  157 us (98%)
  local copies, waits for them, and re-layouts  3.97 us (2%)
    pallas_call x1, Pallas kernels, layer(): pl.pallas_call(functools.partial(layer_kernel, planes, lags), out_shape=j...  157 us

profile of v2, /device:TPU:0, one launch (start us, length us, event | category | flops | bytes accessed | tf_op | source)
XLA Modules:
  0.0 160.7 jit_solution(2449464808209530025)
XLA Ops:
  0.0 1.3 broadcast_in_dim.15.base_in
  1.3 156.7 %shard_map.154 = bf16[192,4096]{1,0:T(8,128)(2,1)} custom-call(bf16[192,4096]{1,0:T(8,128)(2,1)} %tokens.1, f32[1,4096]{1,0:T(1,128)} %bitcast.3, bf16[256,512]{1,0:T(8,128)(2,1)} %val_w.1, bf16[256,512]{1,0:T(8,128)(2,1)} %gate_w.1, bf16[256,768]{1,0:T(8,128)(2,1)} %rgate_w.1, bf16[256,768]{1,0:T(8,128)(2,1)} %rin_w.1, bf16[31,512]{1,0:T(8,128)(2,1)} %taps_in.1, ...), custom_call_target="tpu_custom_call" | custom-call | tf_op jit(solution)/shard_map/pallas_call | solution.py:796
  158.0 2.7 %copy.18 = bf16[192,4096]{1,0:T(8,128)(2,1)} copy(bf16[192,4096]{1,0:T(8,128)(2,1)} %shard_map.154) | data formatting | bytes 3145728

commit v3 on v2

--- a/solution.py
+++ b/solution.py
@@ -313,9 +313,9 @@
                 here, sem = self.take(origin, piece, when)
                 self.mail.send(here, here, sem, on, when)
 
-    def settle(self, k, piece):
+    def settle(self, k, piece, when=True):
         for origin, there, _, more in self.ways(k):
-            self.take(origin, piece, jnp.logical_and(there, jnp.logical_not(more)))
+            self.take(origin, piece, there & jnp.logical_not(more) & when)
 
 
 def small_softplus(v):
@@ -333,9 +333,9 @@
     planes, lags, tokens, gain_in, val_w, gate_w, rgate_w, rin_w, taps_in, bias_in, cgain_in, staps_in,
     dmap_in, imap_in, base_in, jump_in, ocw, orw,
     out, x_ref, gain, rin_s, rgate_s, wr, wc, taps, bias, cgain, staps, dmap, imap, rbase, jump, jb, cpar, rpar,
-    ld, xall, rwall, cwall, projr, jall, wz, wp, yall, cbuf, gext, rext, filt, dec, inf, maps, stat,
+    ld, xall, rwall, cwall, projr, jall, wz, wp, yall, yrest, cacc, cbuf, gext, rext, filt, dec, inf, maps, stat,
     st_all, carry, cr_all,
-    send, rx, rpx, rwr, rwc, zr, zc, zo, rj, ry, rp, rv, rq, rw, rh, rs, rc, ls, lr,
+    send, rx, rpx, rwr, rwc, zr, zc, zo, rj, ry, rp, rv, rq, re, rf, rw, rh, rs, rc, ls, lr,
 ):
     me = Spot(planes)
     mail = Mail(send)
@@ -345,11 +345,13 @@
     length = xall.shape[0]
     cw, rwid = gext.shape[1], rpar.shape[1]
     seg = length // SEGMENTS
+    lane_seg = dec.shape[1] // SEGMENTS
     top = gext.shape[0] - length
     rtop = rext.shape[0] - length
     fold = dec.shape[0]
     part = planes // 2
-    width = yall.shape[1] // 8
+    major = rwid // 128 * 128
+    minor = rwid - major
     mine = me.q * 2 + me.c
     others = (me.qx, me.qy, me.qd)
     pieces = (me.q,) + others
@@ -373,10 +375,12 @@
         got_conv.append(load(val_w.at[:, pl.ds(q * cw, cw)], wc.at[q, :, pl.ds(0, cw)]))
         got_conv.append(load(gate_w.at[:, pl.ds(q * cw, cw)], wc.at[q, :, pl.ds(cw, cw)]))
     got_out = []
+    got_out.append(load(ocw, wz.at[me.z, pl.ds(0, 4 * cw)]))
     for q in range(4):
-        at = q * (cw + rwid)
-        got_out.append(load(ocw.at[pl.ds(q * cw, cw)], wz.at[me.z, pl.ds(at, cw)]))
-        got_out.append(load(orw.at[pl.ds(q * rwid, rwid)], wz.at[me.z, pl.ds(at + cw, rwid)]))
+        at = 4 * cw + q * major
+        got_out.append(load(orw.at[pl.ds(q * rwid, major)], wz.at[me.z, pl.ds(at, major)]))
+        at = 4 * (cw + major) + q * minor
+        got_out.append(load(orw.at[pl.ds(q * rwid + major, minor)], wz.at[me.z, pl.ds(at, minor)]))
     got_jump = [load(jump_in, jump)]
     got_small = [
         load(src, dst)
@@ -534,13 +538,16 @@
 
     @pl.loop(0, SEGMENTS)
     def _(n):
-        i = SEGMENTS - 1 - n
+        step = (n + 1) // 2
+        ring = (me.q // 2 + step % 4 // 2) % 2 * 2 + (me.q % 2 + step % 2) % 2
+        i = jnp.where(n == SEGMENTS - 1, 2 * me.q, 2 * ring + n % 2)
+        i = jnp.where(n == 0, 2 * me.q + 1, i)
 
         @pl.when(jnp.logical_and(i == 0, me.has_down))
         def _():
             mail.arrived(rext.at[pl.ds(0, rtop)], rh.at[0], me.partner)
 
-        @pl.when(jnp.logical_and(i % 2 == 1, i // 2 != me.q))
+        @pl.when(jnp.logical_and(n % 2 == 1, n < SEGMENTS - 1))
         def _():
             mail.arrived(jall.at[i // 2], rj.at[i // 2], me.partner)
 
@@ -559,13 +566,14 @@
         inflow = jnp.sqrt(minus_expm1(2.0 * log_decay)) * admit * smooth.astype(f32)
         for f in range(fold):
             w = min(128, rwid - f * 128)
-            dec[f, pl.ds(base, seg), pl.ds(0, w)] = decay[:, f * 128 : f * 128 + w]
-            inf[f, pl.ds(base, seg), pl.ds(0, w)] = inflow[:, f * 128 : f * 128 + w]
+            spot = pl.ds(pl.multiple_of(i * lane_seg, 8), seg)
+            dec[f, spot, pl.ds(0, w)] = decay[:, f * 128 : f * 128 + w]
+            inf[f, spot, pl.ds(0, w)] = inflow[:, f * 128 : f * 128 + w]
 
     def one(i, held):
         after = []
         for f in range(fold):
-            at = pl.ds(i, SEGMENTS, stride=seg)
+            at = pl.ds(i, SEGMENTS, stride=lane_seg)
             d = dec.at[f][at, :]
             product, state = held[2 * f] * d, held[2 * f + 1] * d + inf.at[f][at, :]
             dec.at[f][at, :] = product
@@ -602,40 +610,65 @@
         for i in range(SEGMENTS):
             entering.append(held)
             held = ends[2 * f][i : i + 1] * held + ends[2 * f + 1][i : i + 1]
-    own_at = pl.multiple_of(mine * width, 128)
-    for i in range(SEGMENTS):
-        here = pl.ds(i * seg, seg)
-        state = [dec[f, here] * entering[f * SEGMENTS + i] + inf[f, here] for f in range(fold)]
+    placed = me.c * 4 + me.q
+
+    def rec_result(i):
+        here, there = pl.ds(i * seg, seg), pl.ds(i * lane_seg, seg)
+        state = [dec[f, there] * entering[f * SEGMENTS + i] + inf[f, there] for f in range(fold)]
         state = jnp.concatenate(state, axis=1)[:, :rwid]
-        result = gelu(projr[here, pl.ds(rwid, rwid)].astype(f32)) * state
-        fill = jnp.zeros((seg, width - cw - rwid), f32)
-        yall[here, pl.ds(pl.multiple_of(own_at + cw, 128), width - cw)] = jnp.concatenate([result, fill], axis=1).astype(bf16)
-
-    part_length = length // rv.shape[1]
-
-    def gather(lane, lanes, recv, recv_pair):
+        result = (gelu(projr[here, pl.ds(rwid, rwid)].astype(f32)) * state).astype(bf16)
+        yall[here, pl.ds(pl.multiple_of(8 * cw + placed * major, 128), major)] = result[:, :major]
+        return result[:, major:]
+
+    for i in range(SEGMENTS // 2):
+        pair = jnp.concatenate([rec_result(i), rec_result(i + SEGMENTS // 2)], axis=1)
+        yrest[pl.ds(i * seg, seg), pl.ds(pl.multiple_of(placed * 2 * minor, 128), 2 * minor)] = pair
+
+    def gather(buffer, lane, lanes, recv, recv_pair):
+        tall_part = buffer.shape[0] // recv.shape[1]
+
         def slot(q, c, h):
-            spot = pl.ds(pl.multiple_of((q * 2 + c) * width + lane, 128), lanes)
-            return yall.at[pl.ds(h * part_length, part_length), spot]
+            spot = pl.ds(pl.multiple_of(lane + (c * 4 + q) * lanes, 128), lanes)
+            return buffer.at[pl.ds(h * tall_part, tall_part), spot]
 
         return PlaneGather(me, mail, slot, recv, recv_pair)
 
-    vg = gather(cw, width - cw, rv, rq)
-    vg.start()
-    for k in range(1, planes):
+    mg = gather(yall, 8 * cw, major, rv, rq)
+    eg = gather(yrest, 0, 2 * minor, re, rf)
+    yg = gather(yall, 0, cw, ry, rp)
+    mg.start()
+    eg.start()
+    for k in range(1, last):
         for p in pieces:
             cl.settle(k, p)
+    plane_depth = 4 * depth
+    is_last = (me.z == last).astype(jnp.int32)
+
+    def conv_product(at, begin, size):
+        deep = pl.ds(pl.multiple_of(begin, plane_depth), size)
+        return jnp.dot(xall[at, deep], cwall[deep], preferred_element_type=f32)
 
     @pl.loop(0, 4)
     def _(i):
         at = pl.ds(pl.multiple_of(i * tile, tile), tile)
-        product = jnp.dot(xall[at], cwall[...], preferred_element_type=f32).astype(bf16).astype(f32)
+        cacc[at] = conv_product(at, is_last * plane_depth, last * plane_depth)
+
+    for i in range(mg.half):
+        mg.first(i)
+    for p in parts:
+        ol.relay(1, p)
+    for p in pieces:
+        cl.settle(last, p)
+
+    @pl.loop(0, 4)
+    def _(i):
+        at = pl.ds(pl.multiple_of(i * tile, tile), tile)
+        product = cacc[at] + conv_product(at, (1 - is_last) * last * plane_depth, plane_depth)
+        product = product.astype(bf16).astype(f32)
         glu = (product[:, :cw] * jax.nn.sigmoid(product[:, cw:])).astype(bf16).astype(f32)
         gext[pl.ds(pl.multiple_of(i * tile + top, 8), tile)] = glu
 
     mail.send(gext.at[pl.ds(length, top)], gext.at[pl.ds(0, top)], rh.at[1], me.up, me.has_up)
-    for p in parts:
-        ol.relay(1, p)
     strips = length // 64
 
     def filter_strip(n):
@@ -648,9 +681,14 @@
         base = pl.multiple_of(i * 64, 8)
         window = gext[pl.ds(base, 64 + top)]
         total = jnp.zeros((64, cw), f32) + cpar[pl.ds(c_lags + 1, 1), :]
-        for k in range(c_lags + 1):
-            begin = top - c_lags + k
-            total = total + cpar[pl.ds(k, 1), :] * window[begin : begin + 64]
+        for r in range(8):
+            ks = [k for k in range(c_lags + 1) if (top - c_lags + k) % 8 == r]
+            span = 64 + (8 if r else 0)
+            shifted = jnp.zeros((span, cw), f32)
+            for k in ks:
+                begin = (top - c_lags + k) // 8 * 8
+                shifted = shifted + cpar[pl.ds(k, 1), :] * window[begin : begin + span]
+            total = total + shifted[r : r + 64]
         filt[pl.ds(base, 64)] = total
         part_sum = jnp.sum(total, axis=1, keepdims=True)
         off = total - part_sum * (1.0 / cw)
@@ -658,16 +696,14 @@
         spread = jnp.sum(off * off, axis=1, keepdims=True)
         stat[pl.ds(base, 64)] = jnp.where(lane == 0, part_sum, spread)
 
-    pl.loop(0, strips // 4)(filter_strip)
-    vg.first(0)
-    pl.loop(strips // 4, strips)(filter_strip)
+    pl.loop(0, strips)(filter_strip)
 
     packed = stat[...].T
     st_all[mine] = packed[0:2]
     for device in mates:
         mail.send(st_all.at[mine], st_all.at[mine], rs.at[mine], device)
-    for i in range(1, vg.half):
-        vg.first(i)
+    for i in range(eg.half):
+        eg.first(i)
 
     for k in range(1, 8):
         d = (mine + k) % 8
@@ -687,85 +723,107 @@
         here = pl.ds(pl.multiple_of(i * seg, 16), seg)
         pair = stat[here]
         v = (filt[here] - pair[:, 0:1]) * pair[:, 1:2] * cpar[pl.ds(c_lags + 2, 1), :]
-        yall[here, pl.ds(own_at, cw)] = (v * jax.nn.sigmoid(v)).astype(bf16)
-
-    yg = gather(0, cw, ry, rp)
+        yall[here, pl.ds(pl.multiple_of(placed * cw, 128), cw)] = (v * jax.nn.sigmoid(v)).astype(bf16)
+
     yg.start()
-    vg.second()
-    for i in range(yg.half):
-        yg.first(i)
     for k in range(2, last):
         for p in parts:
             ol.relay(k, p)
+    mg.second()
+    eg.second()
+    for i in range(yg.half):
+        yg.first(i)
+    mg.third()
+    eg.third()
+    mg.last(pieces)
+    eg.last(pieces)
+    rest_at = 8 * (cw + major)
+
+    @pl.loop(0, SEGMENTS // 2)
+    def _(i):
+        values = yrest[pl.ds(pl.multiple_of(i * seg, 16), seg)]
+        low = [values[:, j * 2 * minor : j * 2 * minor + minor] for j in range(8)]
+        high = [values[:, j * 2 * minor + minor : (j + 1) * 2 * minor] for j in range(8)]
+        for begin, chosen in ((0, low), (length // 2, high)):
+            here = pl.ds(pl.multiple_of(begin + i * seg, 16), seg)
+            yall[here, pl.ds(rest_at, 8 * minor)] = jnp.concatenate(chosen, axis=1)
+
     for k in range(1, last):
         for p in parts:
             ol.settle(k, p)
-    vg.third()
     yg.second()
     yg.third()
-    vg.last(pieces)
     yg.last(pieces)
 
-    used, cols = cw + rwid, wz.shape[2]
-    tile_rows = length // 8
+    cols = wz.shape[2]
     upward = me.z < part
-
-    def multiply(d, k):
-        here = pl.ds(pl.multiple_of(d * tile_rows, 16), tile_rows)
-        total = jnp.zeros((tile_rows, cols), f32)
-        for q in range(4):
-            for c, block in ((me.c, wz.at[me.c * part + k]), (1 - me.c, wp.at[k])):
-                left = yall[here, pl.ds(pl.multiple_of((q * 2 + c) * width, 128), width)]
-                total = total + jnp.dot(
-                    left[:, :used], block[pl.ds(q * used, used)], preferred_element_type=f32
-                )
-        cbuf[d, k] = total.astype(bf16)
+    far = last - me.z
+    far_mine = far // part == me.c
+
+    def multiply(q, k):
+        here = pl.ds(pl.multiple_of(q * 2 * rows, 16), 2 * rows)
+        total = jnp.zeros((2 * rows, cols), f32)
+        for c, block in ((me.c, wz.at[me.c * part + k]), (1 - me.c, wp.at[k])):
+            begin = 0
+            for at, lanes in ((0, 4 * cw), (8 * cw, 4 * major), (rest_at, 4 * minor)):
+                left = yall[here, pl.ds(pl.multiple_of(at + c * lanes, 128), lanes)]
+                total = total + jnp.dot(left, block[pl.ds(begin, lanes)], preferred_element_type=f32)
+                begin = begin + lanes
+        total = total.astype(bf16)
+        for c in range(2):
+            cbuf[q * 2 + c, k] = total[c * rows : (c + 1) * rows]
 
     def place(q, c, k):
         return out.at[:, pl.ds(pl.multiple_of(((c * part + k) * 4 + q) * cols, 128), cols)]
 
-    def target(i):
-        flip = 3 - i // 2
-        q = (me.q // 2 + flip // 2) % 2 * 2 + (me.q % 2 + flip % 2) % 2
-        return q, (me.c + 1 + i) % 2
-
-    def parcel(i, k):
-        q, c = target(i)
+    def mate_of(i):
+        flip = 3 - i
+        return (me.q // 2 + flip // 2) % 2 * 2 + (me.q % 2 + flip % 2) % 2
+
+    def parcel(q, c, k):
         return pltpu.make_async_remote_copy(
-            src_ref=cbuf.at[q * 2 + c, k], dst_ref=place(me.q, me.c, k), send_sem=ls.at[i, k],
+            src_ref=cbuf.at[q * 2 + c, k], dst_ref=place(me.q, me.c, k), send_sem=ls.at[q * 2 + c, k],
             recv_sem=lr.at[mine, k], device_id=me.at(me.z * 4 + q, c), device_id_type=MESH,
         )
 
     def kept(k):
-        return pltpu.make_async_copy(cbuf.at[mine, k], place(me.q, me.c, k), ls.at[7, k])
-
-    def round_of(n):
-        k = jnp.where(upward, n, part - 1 - n)
-
-        @pl.loop(0, 7)
-        def _(i):
-            q, c = target(i)
-            multiply(q * 2 + c, k)
-            parcel(i, k).start()
-
-        multiply(mine, k)
-        kept(k).start()
+        return pltpu.make_async_copy(cbuf.at[mine, k], place(me.q, me.c, k), ls.at[mine, k])
 
     for n in range(part):
         k = jnp.where(upward, n, part - 1 - n)
         if n == part - 1:
             for p in parts:
-                ol.settle(last, p)
+                ol.settle(last, p, far_mine)
         for p in parts:
             mail.arrived(wp.at[k, pl.ds(p * tall, tall)], rw.at[k, p], me.partner)
-        round_of(n)
-
-    @pl.loop(0, 7)
+
+        @pl.loop(0, 3)
+        def _(i):
+            q = mate_of(i)
+            multiply(q, k)
+            for c in (me.c, 1 - me.c):
+                parcel(q, c, k).start()
+
+        multiply(me.q, k)
+        parcel(me.q, 1 - me.c, k).start()
+        kept(k).start()
+
+    for p in parts:
+        ol.settle(last, p, jnp.logical_not(far_mine))
+
+    @pl.loop(0, 4)
     def _(i):
-        q, c = target(i)
+        q = mate_of(i)
         for k in range(part):
-            mail.arrived(place(q, c, k), lr.at[q * 2 + c, k], me.partner)
-            parcel(i, k).wait_send()
+            mail.arrived(place(q, 1 - me.c, k), lr.at[q * 2 + 1 - me.c, k], me.partner)
+            parcel(q, 1 - me.c, k).wait_send()
+
+    @pl.loop(0, 3)
+    def _(i):
+        q = mate_of(i)
+        for k in range(part):
+            mail.arrived(place(q, me.c, k), lr.at[q * 2 + me.c, k], me.partner)
+            parcel(q, me.c, k).wait_send()
 
     for k in range(part):
         kept(k).wait()
@@ -778,7 +836,7 @@
     depth = rin_w.shape[0]
     cw, rwid = val_w.shape[1] // 4, rin_w.shape[1] // 4
     used, cols = cw + rwid, ocw.shape[1]
-    width = used + -used % 128
+    minor = rwid % 128
     fold = (rwid + 127) // 128
     f32, bf16 = jnp.float32, jnp.bfloat16
     dma = pltpu.SemaphoreType.DMA
@@ -812,21 +870,23 @@
             vmem(4, jump.shape[0] // 2, 2 * rwid),
             vmem(planes, 4 * used, cols),
             vmem(part, 4 * used, cols),
-            vmem(length, 8 * width),
+            vmem(length, 8 * used),
+            vmem(length // 2, 16 * minor),
+            wide(length, 2 * cw),
             vmem(8, part, rows, cols),
             wide(top + length, cw),
             wide(rtop + length, rwid),
             wide(length, cw),
-            wide(fold, length, 128),
-            wide(fold, length, 128),
+            wide(fold, length + 8 * SEGMENTS, 128),
+            wide(fold, length + 8 * SEGMENTS, 128),
             vmem(rwid, 2 * fold * 128),
             wide(length, 128),
             wide(8, 2, length),
             wide(8, 128),
             wide(planes, 8, 128),
-            dma((160 + 20 * planes,)), dma((4, 4)), dma((4, 4)), dma((4,)), dma((4,)),
+            dma((180 + 20 * planes,)), dma((4, 4)), dma((4, 4)), dma((4,)), dma((4,)),
             dma((planes, 4)), dma((planes, 4)), dma((planes, OUT_PARTS)), dma((4,)),
-            dma((4, 4)), dma((4, 4)), dma((4, 4)), dma((4, 4)), dma((part, OUT_PARTS)),
+            dma((4, 4)), dma((4, 4)), dma((4, 4)), dma((4, 4)), dma((4, 2)), dma((4, 2)), dma((part, OUT_PARTS)),
             dma((2,)), dma((8,)), dma((planes,)), dma((8, part)), dma((8, part)),
         ],
         compiler_params=pltpu.CompilerParams(

time: 161 us -> 168 us (1.043)
  the two profiles are of different devices: /device:TPU:0 before, /device:TPU:25 now
where the time goes in v3:
time: 168 us
  Pallas kernels  164 us (98%)
  local copies, waits for them, and re-layouts  3.97 us (2%)
    pallas_call x1, Pallas kernels, layer(): pl.pallas_call(functools.partial(layer_kernel, planes, lags), out_shape=j...  164 us

profile of v3, /device:TPU:25, one launch (start us, length us, event | category | flops | bytes accessed | tf_op | source)
XLA Modules:
  0.0 168.1 jit_solution(15757520907104220094)
XLA Ops:
  0.0 1.3 broadcast_in_dim.15.base_in
  1.3 164.1 %shard_map.154 = bf16[192,4096]{1,0:T(8,128)(2,1)} custom-call(bf16[192,4096]{1,0:T(8,128)(2,1)} %tokens.1, f32[1,4096]{1,0:T(1,128)} %bitcast.3, bf16[256,512]{1,0:T(8,128)(2,1)} %val_w.1, bf16[256,512]{1,0:T(8,128)(2,1)} %gate_w.1, bf16[256,768]{1,0:T(8,128)(2,1)} %rgate_w.1, bf16[256,768]{1,0:T(8,128)(2,1)} %rin_w.1, bf16[31,512]{1,0:T(8,128)(2,1)} %taps_in.1, ...), custom_call_target="tpu_custom_call" | custom-call | tf_op jit(solution)/shard_map/pallas_call | solution.py:854
  165.4 2.7 %copy.18 = bf16[192,4096]{1,0:T(8,128)(2,1)} copy(bf16[192,4096]{1,0:T(8,128)(2,1)} %shard_map.154) | data formatting | bytes 3145728

commit v4 on v3

--- a/solution.py
+++ b/solution.py
@@ -289,8 +289,8 @@
     def own(self, piece, src, up=True, down=True):
         me = self.me
         for wanted, has, device in ((up, me.has_up, me.up), (down, me.has_down, me.down)):
-            if wanted:
-                self.mail.send(src, self.slot(me.z, piece), self.recv.at[me.z, piece], device, has)
+            if wanted is not False:
+                self.mail.send(src, self.slot(me.z, piece), self.recv.at[me.z, piece], device, has & wanted)
 
     def ways(self, k):
         me = self.me
@@ -313,6 +313,15 @@
                 here, sem = self.take(origin, piece, when)
                 self.mail.send(here, here, sem, on, when)
 
+    def await_up(self, k, piece):
+        origin, there, _, more = self.ways(k)[0]
+        return self.take(origin, piece, there & more)
+
+    def forward_up(self, k, piece):
+        origin, there, on, more = self.ways(k)[0]
+        here, sem = self.slot(origin, piece), self.recv.at[origin, piece]
+        self.mail.send(here, here, sem, on, there & more)
+
     def settle(self, k, piece, when=True):
         for origin, there, _, more in self.ways(k):
             self.take(origin, piece, there & jnp.logical_not(more) & when)
@@ -333,7 +342,7 @@
     planes, lags, tokens, gain_in, val_w, gate_w, rgate_w, rin_w, taps_in, bias_in, cgain_in, staps_in,
     dmap_in, imap_in, base_in, jump_in, ocw, orw,
     out, x_ref, gain, rin_s, rgate_s, wr, wc, taps, bias, cgain, staps, dmap, imap, rbase, jump, jb, cpar, rpar,
-    ld, xall, rwall, cwall, projr, jall, wz, wp, yall, yrest, cacc, cbuf, gext, rext, filt, dec, inf, maps, stat,
+    ld, xall, rwall, cwall, projr, jall, wz, wp, yall, yrest, cacc, cbuf, gext, rext, filt, dec, inf, maps, ft,
     st_all, carry, cr_all,
     send, rx, rpx, rwr, rwc, zr, zc, zo, rj, ry, rp, rv, rq, re, rf, rw, rh, rs, rc, ls, lr,
 ):
@@ -412,8 +421,8 @@
     cl = Line(me, mail, planes, of_rows(cwall), zc)
     ol = Line(me, mail, planes, lambda origin, p: wz.at[origin, pl.ds(p * tall, tall)], zo, theirs_too)
 
-    def out_own(p):
-        ol.own(p, wz.at[me.z, pl.ds(p * tall, tall)])
+    def out_own(p, up=True, down=True):
+        ol.own(p, wz.at[me.z, pl.ds(p * tall, tall)], up, down)
 
     for q in others:
         mail.send(wr.at[q], rl.slot(me.z, me.q), rwr.at[me.q], me.mate(q))
@@ -470,7 +479,7 @@
         return moved
 
     rpar[pl.ds(0, s_lags + 1)] = own_rec(staps[:, wide_lanes].astype(f32))
-    rpar[pl.ds(s_lags + 1, 1)] = own_rec(RATE_SCALE * small_softplus(-rbase[:, wide_lanes]))
+    rpar[pl.ds(s_lags + 1, 1)] = own_rec(RATE_SCALE * small_softplus(-rbase[wide_lanes][None]))
 
     maps[...] = jnp.zeros_like(maps)
     size = dmap.shape[1]
@@ -517,17 +526,17 @@
         project_rec((me.q // 2 + i // 2) % 2 * 2 + (me.q % 2 + i % 2) % 2)
 
     for n, p in enumerate(pieces):
-        cl.relay(1, p, n < 2, True)
+        cl.relay(1, p, n < 1, True)
     xg.third()
     xg.last(pieces[3:])
     project_rec(me.qd)
 
     mail.send(rext.at[pl.ds(length, rtop)], rext.at[pl.ds(0, rtop)], rh.at[0], me.up, me.has_up)
-    for p in pieces[2:]:
+    for p in pieces[1:3]:
         cl.relay(1, p, True, False)
     for k in range(2, last):
-        for n, p in enumerate(pieces):
-            cl.relay(k, p, n < 1, True)
+        for p in pieces:
+            cl.relay(k, p, False, True)
 
     @pl.when(jnp.logical_not(me.has_down))
     def _():
@@ -592,11 +601,13 @@
         carry[pl.ds(2 * f + 1, 1)] = state
     for k in range(1, planes):
         mail.send(carry, cr_all.at[me.z], rc.at[me.z], lined[k - 1], me.z + k < planes)
+    early = me.z < planes - 2
+    cl.relay(1, pieces[3], True, False)
     for k in range(2, last):
-        for p in pieces[1:]:
+        for p in pieces[:2]:
             cl.relay(k, p, True, False)
     for p in parts[2:]:
-        out_own(p)
+        out_own(p, early, True)
 
     for k in range(1, planes):
         z = me.z - k
@@ -641,6 +652,8 @@
     for k in range(1, last):
         for p in pieces:
             cl.settle(k, p)
+        for p in pieces[2:] if k > 1 else ():
+            cl.await_up(k, p)
     plane_depth = 4 * depth
     is_last = (me.z == last).astype(jnp.int32)
 
@@ -653,22 +666,33 @@
         at = pl.ds(pl.multiple_of(i * tile, tile), tile)
         cacc[at] = conv_product(at, is_last * plane_depth, last * plane_depth)
 
+    middle = me.has_up & me.has_down
+
+    def finish_conv(when):
+        @pl.when(when)
+        def _():
+            @pl.loop(0, 4)
+            def _(i):
+                at = pl.ds(pl.multiple_of(i * tile, tile), tile)
+                product = cacc[at] + conv_product(at, (1 - is_last) * last * plane_depth, plane_depth)
+                product = product.astype(bf16).astype(f32)
+                glu = (product[:, :cw] * jax.nn.sigmoid(product[:, cw:])).astype(bf16).astype(f32)
+                gext[pl.ds(pl.multiple_of(i * tile + top, 8), tile)] = glu
+
+        tail_rows = gext.at[pl.ds(length, top)]
+        mail.send(tail_rows, gext.at[pl.ds(0, top)], rh.at[1], me.up, me.has_up & when)
+
+    finish_conv(middle)
+    for k in range(2, last):
+        for p in pieces[2:]:
+            cl.forward_up(k, p)
+    for p in parts[2:]:
+        out_own(p, jnp.logical_not(early), False)
     for i in range(mg.half):
         mg.first(i)
-    for p in parts:
-        ol.relay(1, p)
     for p in pieces:
         cl.settle(last, p)
-
-    @pl.loop(0, 4)
-    def _(i):
-        at = pl.ds(pl.multiple_of(i * tile, tile), tile)
-        product = cacc[at] + conv_product(at, (1 - is_last) * last * plane_depth, plane_depth)
-        product = product.astype(bf16).astype(f32)
-        glu = (product[:, :cw] * jax.nn.sigmoid(product[:, cw:])).astype(bf16).astype(f32)
-        gext[pl.ds(pl.multiple_of(i * tile + top, 8), tile)] = glu
-
-    mail.send(gext.at[pl.ds(length, top)], gext.at[pl.ds(0, top)], rh.at[1], me.up, me.has_up)
+    finish_conv(jnp.logical_not(middle))
     strips = length // 64
 
     def filter_strip(n):
@@ -690,20 +714,21 @@
                 shifted = shifted + cpar[pl.ds(k, 1), :] * window[begin : begin + span]
             total = total + shifted[r : r + 64]
         filt[pl.ds(base, 64)] = total
-        part_sum = jnp.sum(total, axis=1, keepdims=True)
-        off = total - part_sum * (1.0 / cw)
-        lane = lax.broadcasted_iota(jnp.int32, (64, 128), 1)
-        spread = jnp.sum(off * off, axis=1, keepdims=True)
-        stat[pl.ds(base, 64)] = jnp.where(lane == 0, part_sum, spread)
 
     pl.loop(0, strips)(filter_strip)
 
-    packed = stat[...].T
-    st_all[mine] = packed[0:2]
+    turned = filt[...].T
+    ft[...] = turned
+    part_sum = jnp.sum(turned, axis=0, keepdims=True)
+    off = turned - part_sum * (1.0 / cw)
+    st_all[mine, pl.ds(0, 1)] = part_sum
+    st_all[mine, pl.ds(1, 1)] = jnp.sum(off * off, axis=0, keepdims=True)
     for device in mates:
         mail.send(st_all.at[mine], st_all.at[mine], rs.at[mine], device)
     for i in range(eg.half):
         eg.first(i)
+    for p in parts:
+        ol.relay(1, p)
 
     for k in range(1, 8):
         d = (mine + k) % 8
@@ -715,26 +740,19 @@
         shift = st_all[d, 0:1, :] * (1.0 / cw) - mean
         spread = spread + st_all[d, 1:2, :] + cw * shift * shift
     scale = lax.rsqrt(spread * (1.0 / (8 * cw)) + 1e-05)
-    row = lax.broadcasted_iota(jnp.int32, (128, length), 0)
-    stat[...] = jnp.where(row == 0, mean, scale).T
-
-    @pl.loop(0, SEGMENTS)
-    def _(i):
-        here = pl.ds(pl.multiple_of(i * seg, 16), seg)
-        pair = stat[here]
-        v = (filt[here] - pair[:, 0:1]) * pair[:, 1:2] * cpar[pl.ds(c_lags + 2, 1), :]
-        yall[here, pl.ds(pl.multiple_of(placed * cw, 128), cw)] = (v * jax.nn.sigmoid(v)).astype(bf16)
-
+    gain_col = jnp.broadcast_to(cpar[pl.ds(c_lags + 2, 1), :], (8, cw)).T[:, 0:1]
+    v = (ft[...] - mean) * scale * gain_col
+    yall[:, pl.ds(pl.multiple_of(placed * cw, 128), cw)] = (v * jax.nn.sigmoid(v)).T.astype(bf16)
     yg.start()
+    mg.second()
+    eg.second()
+    mg.third()
+    eg.third()
+    for i in range(yg.half):
+        yg.first(i)
     for k in range(2, last):
         for p in parts:
             ol.relay(k, p)
-    mg.second()
-    eg.second()
-    for i in range(yg.half):
-        yg.first(i)
-    mg.third()
-    eg.third()
     mg.last(pieces)
     eg.last(pieces)
     rest_at = 8 * (cw + major)
@@ -860,7 +878,7 @@
             vmem(rows, width_in), wide(1, width_in), vmem(*rin_w.shape), vmem(*rgate_w.shape),
             vmem(4, depth, 2 * rwid), vmem(4, depth, 2 * cw),
             vmem(*taps.shape), wide(1, 4 * cw), wide(1, 4 * cw), vmem(*staps.shape),
-            vmem(*dmap.shape), vmem(*imap.shape), wide(1, 4 * rwid), wide(*jump.shape),
+            vmem(*dmap.shape), vmem(*imap.shape), wide(4 * rwid), wide(*jump.shape),
             vmem(4, jump.shape[0] // 2, 2 * rwid), wide(lags[0] + 3 + -(lags[0] + 3) % 8, cw), wide(8, rwid),
             dma((32,)),
             vmem(length, width_in),
@@ -880,7 +898,7 @@
             wide(fold, length + 8 * SEGMENTS, 128),
             wide(fold, length + 8 * SEGMENTS, 128),
             vmem(rwid, 2 * fold * 128),
-            wide(length, 128),
+            wide(cw, length),
             wide(8, 2, length),
             wide(8, 128),
             wide(planes, 8, 128),
@@ -894,7 +912,7 @@
         ),
     )(
         tokens, norm_gain[None], val_w, gate_w, rgate_w, rin_w, taps, bias[None], cgain[None], staps,
-        dmap, imap, rbase[None], jump, ocw, orw,
+        dmap, imap, rbase, jump, ocw, orw,
     )
 
 

time: 168 us -> 151 us (0.90)
  the two profiles are of different devices: /device:TPU:25 before, /device:TPU:0 now
where the time goes in v4:
time: 151 us
  Pallas kernels  148 us (98%)
  local copies, waits for them, and re-layouts  2.7 us (2%)
    pallas_call x1, Pallas kernels, layer(): pl.pallas_call(functools.partial(layer_kernel, planes, lags), out_shape=j...  148 us

profile of v4, /device:TPU:0, one launch (start us, length us, event | category | flops | bytes accessed | tf_op | source)
XLA Modules:
  0.0 150.9 jit_solution(11401604360965908493)
XLA Ops:
  0.0 148.2 %shard_map.154 = bf16[192,4096]{1,0:T(8,128)(2,1)} custom-call(bf16[192,4096]{1,0:T(8,128)(2,1)} %tokens.1, f32[1,4096]{1,0:T(1,128)} %bitcast.3, bf16[256,512]{1,0:T(8,128)(2,1)} %val_w.1, bf16[256,512]{1,0:T(8,128)(2,1)} %gate_w.1, bf16[256,768]{1,0:T(8,128)(2,1)} %rgate_w.1, bf16[256,768]{1,0:T(8,128)(2,1)} %rin_w.1, bf16[31,512]{1,0:T(8,128)(2,1)} %taps_in.1, ...), custom_call_target="tpu_custom_call" | custom-call | tf_op jit(solution)/shard_map/pallas_call | solution.py:872
  148.2 2.7 %copy.18 = bf16[192,4096]{1,0:T(8,128)(2,1)} copy(bf16[192,4096]{1,0:T(8,128)(2,1)} %shard_map.154) | data formatting | bytes 3145728

commit v5 on v4

--- a/solution.py
+++ b/solution.py
@@ -258,16 +258,18 @@
             for q, part in ((self.me.qx, self.half + i), (self.me.qy, i)):
                 self.share(q, part, self.took(q, part))
 
-    def third(self):
-        for i in range(self.half):
-            for part in (i, self.half + i):
-                self.share(self.me.qd, part, self.took(self.me.qd, part))
+    def third(self, i):
+        for part in (i, self.half + i):
+            self.share(self.me.qd, part, self.took(self.me.qd, part))
+
+    def paired(self, q, part):
+        me = self.me
+        self.mail.arrived(self.slot(q, 1 - me.c, part), self.recv_pair.at[q, part], me.partner)
 
     def last(self, origins):
-        me = self.me
         for q in origins:
             for part in range(self.parts):
-                self.mail.arrived(self.slot(q, 1 - me.c, part), self.recv_pair.at[q, part], me.partner)
+                self.paired(q, part)
 
 
 def minus_expm1(y):
@@ -365,7 +367,11 @@
     others = (me.qx, me.qy, me.qd)
     pieces = (me.q,) + others
     parts = tuple(range(OUT_PARTS))
-    tall = wz.shape[1] // OUT_PARTS
+    tall, half_cols = wz.shape[1] // 2, wz.shape[2] // 2
+
+    def cut(p):
+        return pl.ds(p % 2 * tall, tall), pl.ds(p // 2 * half_cols, half_cols)
+
     last = planes - 1
     mates = [me.at(me.z * 4 + (me.q + dq) % 4, c) for dq in range(4) for c in (me.c, 1 - me.c)][1:]
     lined = [me.at((me.s + 4 * k) % (4 * planes), me.c) for k in range(1, planes)]
@@ -414,15 +420,14 @@
     def theirs_too(origin, piece, when):
         theirs = jnp.logical_and(origin // part != me.c, when)
         place = origin - (1 - me.c) * part
-        rest = pl.ds(piece * tall, tall)
-        mail.send(wz.at[origin, rest], wp.at[place, rest], rw.at[place, piece], me.partner, theirs)
+        mail.send(wz.at[(origin, *cut(piece))], wp.at[(place, *cut(piece))], rw.at[place, piece], me.partner, theirs)
 
     rl = Line(me, mail, planes, of_rows(rwall), zr)
     cl = Line(me, mail, planes, of_rows(cwall), zc)
-    ol = Line(me, mail, planes, lambda origin, p: wz.at[origin, pl.ds(p * tall, tall)], zo, theirs_too)
+    ol = Line(me, mail, planes, lambda origin, p: wz.at[(origin, *cut(p))], zo, theirs_too)
 
     def out_own(p, up=True, down=True):
-        ol.own(p, wz.at[me.z, pl.ds(p * tall, tall)], up, down)
+        ol.own(p, wz.at[(me.z, *cut(p))], up, down)
 
     for q in others:
         mail.send(wr.at[q], rl.slot(me.z, me.q), rwr.at[me.q], me.mate(q))
@@ -450,8 +455,8 @@
         copy.wait()
     for q in others:
         mail.send(wc.at[q], cl.slot(me.z, me.q), rwc.at[me.q], me.mate(q))
+    cl.own(me.q, wc.at[me.q])
     out_own(0)
-    out_own(1)
     kept_here = [mail.local(wr.at[me.q], rl.slot(me.z, me.q)), mail.local(wc.at[me.q], cl.slot(me.z, me.q))]
     for entry in kept_here:
         mail.open.remove(entry)
@@ -495,7 +500,6 @@
         rl.own(q, here)
     for p in pieces:
         rl.relay(1, p)
-    cl.own(me.q, wc.at[me.q])
     for i in range(xg.half):
         xg.first(i)
     for q in others:
@@ -527,7 +531,8 @@
 
     for n, p in enumerate(pieces):
         cl.relay(1, p, n < 1, True)
-    xg.third()
+    for i in range(xg.half):
+        xg.third(i)
     xg.last(pieces[3:])
     project_rec(me.qd)
 
@@ -606,7 +611,7 @@
     for k in range(2, last):
         for p in pieces[:2]:
             cl.relay(k, p, True, False)
-    for p in parts[2:]:
+    for p in parts[1:]:
         out_own(p, early, True)
 
     for k in range(1, planes):
@@ -686,10 +691,9 @@
     for k in range(2, last):
         for p in pieces[2:]:
             cl.forward_up(k, p)
-    for p in parts[2:]:
+    for p in parts[1:]:
         out_own(p, jnp.logical_not(early), False)
-    for i in range(mg.half):
-        mg.first(i)
+    mg.first(0)
     for p in pieces:
         cl.settle(last, p)
     finish_conv(jnp.logical_not(middle))
@@ -725,6 +729,8 @@
     st_all[mine, pl.ds(1, 1)] = jnp.sum(off * off, axis=0, keepdims=True)
     for device in mates:
         mail.send(st_all.at[mine], st_all.at[mine], rs.at[mine], device)
+    for i in range(1, mg.half):
+        mg.first(i)
     for i in range(eg.half):
         eg.first(i)
     for p in parts:
@@ -746,8 +752,9 @@
     yg.start()
     mg.second()
     eg.second()
-    mg.third()
-    eg.third()
+    for g in (mg, eg):
+        for i in range(g.half):
+            g.third(i)
     for i in range(yg.half):
         yg.first(i)
     for k in range(2, last):
@@ -766,86 +773,132 @@
             here = pl.ds(pl.multiple_of(begin + i * seg, 16), seg)
             yall[here, pl.ds(rest_at, 8 * minor)] = jnp.concatenate(chosen, axis=1)
 
+    yg.second()
+    yg.third(0)
     for k in range(1, last):
         for p in parts:
             ol.settle(k, p)
-    yg.second()
-    yg.third()
-    yg.last(pieces)
 
     cols = wz.shape[2]
     upward = me.z < part
     far = last - me.z
     far_mine = far // part == me.c
 
-    def multiply(q, k):
+    def lanes_of(h):
+        return pl.ds(0, cols) if h is None else pl.ds(h * half_cols, half_cols)
+
+    def multiply(q, k, h):
         here = pl.ds(pl.multiple_of(q * 2 * rows, 16), 2 * rows)
-        total = jnp.zeros((2 * rows, cols), f32)
+        total = jnp.zeros((2 * rows, cols if h is None else half_cols), f32)
         for c, block in ((me.c, wz.at[me.c * part + k]), (1 - me.c, wp.at[k])):
             begin = 0
             for at, lanes in ((0, 4 * cw), (8 * cw, 4 * major), (rest_at, 4 * minor)):
                 left = yall[here, pl.ds(pl.multiple_of(at + c * lanes, 128), lanes)]
-                total = total + jnp.dot(left, block[pl.ds(begin, lanes)], preferred_element_type=f32)
+                right = block[pl.ds(begin, lanes), lanes_of(h)]
+                total = total + jnp.dot(left, right, preferred_element_type=f32)
                 begin = begin + lanes
         total = total.astype(bf16)
         for c in range(2):
-            cbuf[q * 2 + c, k] = total[c * rows : (c + 1) * rows]
-
-    def place(q, c, k):
-        return out.at[:, pl.ds(pl.multiple_of(((c * part + k) * 4 + q) * cols, 128), cols)]
+            cbuf[q * 2 + c, k, :, lanes_of(h)] = total[c * rows : (c + 1) * rows]
+
+    def place(q, c, k, h):
+        at = ((c * part + k) * 4 + q) * cols + (0 if h is None else h * half_cols)
+        return out.at[:, pl.ds(pl.multiple_of(at, 128), cols if h is None else half_cols)]
 
     def mate_of(i):
         flip = 3 - i
         return (me.q // 2 + flip // 2) % 2 * 2 + (me.q % 2 + flip % 2) % 2
 
-    def parcel(q, c, k):
+    def parcel(q, c, k, h):
         return pltpu.make_async_remote_copy(
-            src_ref=cbuf.at[q * 2 + c, k], dst_ref=place(me.q, me.c, k), send_sem=ls.at[q * 2 + c, k],
-            recv_sem=lr.at[mine, k], device_id=me.at(me.z * 4 + q, c), device_id_type=MESH,
+            src_ref=cbuf.at[q * 2 + c, k, :, lanes_of(h)], dst_ref=place(me.q, me.c, k, h),
+            send_sem=ls.at[q * 2 + c, k, h or 0], recv_sem=lr.at[mine, k, h or 0],
+            device_id=me.at(me.z * 4 + q, c), device_id_type=MESH,
         )
 
-    def kept(k):
-        return pltpu.make_async_copy(cbuf.at[mine, k], place(me.q, me.c, k), ls.at[mine, k])
-
-    for n in range(part):
-        k = jnp.where(upward, n, part - 1 - n)
-        if n == part - 1:
-            for p in parts:
-                ol.settle(last, p, far_mine)
-        for p in parts:
-            mail.arrived(wp.at[k, pl.ds(p * tall, tall)], rw.at[k, p], me.partner)
-
-        @pl.loop(0, 3)
-        def _(i):
-            q = mate_of(i)
-            multiply(q, k)
-            for c in (me.c, 1 - me.c):
-                parcel(q, c, k).start()
-
-        multiply(me.q, k)
-        parcel(me.q, 1 - me.c, k).start()
-        kept(k).start()
-
+    def kept(k, h):
+        src = cbuf.at[mine, k, :, lanes_of(h)]
+        return pltpu.make_async_copy(src, place(me.q, me.c, k, h), ls.at[mine, k, h or 0])
+
+    def serve(q, k, h):
+        multiply(q, k, h)
+        pl.when(q != me.q)(lambda: parcel(q, me.c, k, h).start())
+        parcel(q, 1 - me.c, k, h).start()
+        pl.when(q == me.q)(lambda: kept(k, h).start())
+
+    def ready(k, ps):
+        for p in ps:
+            mail.arrived(wp.at[(k, *cut(p))], rw.at[k, p], me.partner)
+
+    order = [jnp.where(upward, n, part - 1 - n) for n in range(part)]
+    ready(order[0], parts)
+    for i in range(yg.half):
+        if i:
+            yg.third(i)
+        for q in pieces:
+            yg.paired(q, i)
+            yg.paired(q, yg.half + i)
+
+        @pl.loop(0, 2)
+        def _(n):
+            serve(n * yg.half + i, order[0], None)
+
+    for n in range(1, part - 1):
+        ready(order[n], parts)
+        pl.loop(0, 4)(lambda i: serve(mate_of(i), order[n], None))
+    for h in range(2):
+        halves = parts[2 * h : 2 * h + 2]
+        for p in halves:
+            ol.settle(last, p, far_mine)
+        ready(order[-1], halves)
+        pl.loop(0, 4)(lambda i: serve(mate_of(i), order[-1], h))
     for p in parts:
         ol.settle(last, p, jnp.logical_not(far_mine))
+    rounds = [(k, None) for k in order[:-1]] + [(order[-1], 0), (order[-1], 1)]
 
     @pl.loop(0, 4)
     def _(i):
         q = mate_of(i)
-        for k in range(part):
-            mail.arrived(place(q, 1 - me.c, k), lr.at[q * 2 + 1 - me.c, k], me.partner)
-            parcel(q, 1 - me.c, k).wait_send()
+        for k, h in rounds:
+            mail.arrived(place(q, 1 - me.c, k, h), lr.at[q * 2 + 1 - me.c, k, h or 0], me.partner)
+            parcel(q, 1 - me.c, k, h).wait_send()
 
     @pl.loop(0, 3)
     def _(i):
         q = mate_of(i)
-        for k in range(part):
-            mail.arrived(place(q, me.c, k), lr.at[q * 2 + me.c, k], me.partner)
-            parcel(q, me.c, k).wait_send()
-
-    for k in range(part):
-        kept(k).wait()
+        for k, h in rounds:
+            mail.arrived(place(q, me.c, k, h), lr.at[q * 2 + me.c, k, h or 0], me.partner)
+            parcel(q, me.c, k, h).wait_send()
+
+    for k, h in rounds:
+        kept(k, h).wait()
     mail.finish()
+
+
+def handed_out_kernel(src, dst, held, got, sent):
+    count = got.shape[0]
+    tall = src.shape[0] // count
+    spots = [pl.ds(i * tall, tall) for i in range(count)]
+    taken = [pltpu.make_async_copy(src.at[s], held.at[s], got.at[i]) for i, s in enumerate(spots)]
+    given = [pltpu.make_async_copy(held.at[s], dst.at[s], sent.at[i]) for i, s in enumerate(spots)]
+    for copy in taken:
+        copy.start()
+    for came, goes in zip(taken, given):
+        came.wait()
+        goes.start()
+    for copy in given:
+        copy.wait()
+
+
+def handed_out(result):
+    dma = pltpu.SemaphoreType.DMA
+    return pl.pallas_call(
+        handed_out_kernel,
+        out_shape=jax.ShapeDtypeStruct(result.shape, result.dtype),
+        in_specs=[ANY],
+        out_specs=ANY,
+        scratch_shapes=[pltpu.VMEM(result.shape, result.dtype), dma((6,)), dma((6,))],
+    )(result)
 
 
 def layer(planes, lags, tokens, norm_gain, val_w, gate_w, rgate_w, rin_w, taps, bias, cgain, staps, dmap, imap, rbase, jump, ocw, orw):
@@ -905,7 +958,7 @@
             dma((180 + 20 * planes,)), dma((4, 4)), dma((4, 4)), dma((4,)), dma((4,)),
             dma((planes, 4)), dma((planes, 4)), dma((planes, OUT_PARTS)), dma((4,)),
             dma((4, 4)), dma((4, 4)), dma((4, 4)), dma((4, 4)), dma((4, 2)), dma((4, 2)), dma((part, OUT_PARTS)),
-            dma((2,)), dma((8,)), dma((planes,)), dma((8, part)), dma((8, part)),
+            dma((2,)), dma((8,)), dma((planes,)), dma((8, part, 2)), dma((8, part, 2)),
         ],
         compiler_params=pltpu.CompilerParams(
             collective_id=0, has_side_effects=True, vmem_limit_bytes=60 * 1024 * 1024
@@ -936,10 +989,10 @@
     out_rec_w,
 ):
     lags = (conv_taps.shape[0] - 1, short_taps.shape[0] - 1)
-    return layer(
+    return handed_out(layer(
         planes, lags, tokens, norm_gain, conv_val_w, conv_gate_w, rec_gate_w, rec_in_w, conv_taps, conv_bias,
         conv_gain, short_taps, decay_map, input_map, decay_base, decay_jump, out_conv_w, out_rec_w,
-    )
+    ))
 
 
 def solution(mesh):

time: 151 us -> 153 us (1.013)
  the two profiles are of different devices: /device:TPU:0 before, /device:TPU:30 now
where the time goes in v5:
time: 153 us
  Pallas kernels  153 us (100%)
    pallas_call x1, Pallas kernels, layer(): pl.pallas_call(functools.partial(layer_kernel, planes, lags), out_shape=j...  150 us

profile of v5, /device:TPU:30, one launch (start us, length us, event | category | flops | bytes accessed | tf_op | source)
XLA Modules:
  0.0 152.7 jit_solution(6821928366046903702)
XLA Ops:
  0.0 150.5 %shard_map.154.src = bf16[192,4096]{1,0:T(8,128)(2,1)} custom-call(bf16[192,4096]{1,0:T(8,128)(2,1)} %tokens.1, f32[1,4096]{1,0:T(1,128)} %bitcast.3, bf16[256,512]{1,0:T(8,128)(2,1)} %val_w.1, bf16[256,512]{1,0:T(8,128)(2,1)} %gate_w.1, bf16[256,768]{1,0:T(8,128)(2,1)} %rgate_w.1, bf16[256,768]{1,0:T(8,128)(2,1)} %rin_w.1, bf16[31,512]{1,0:T(8,128)(2,1)} %taps_in.1, ...), custom_call_target="tpu_custom_call" | custom-call | tf_op jit(solution)/shard_map/pallas_call | solution.py:925
  150.5 2.2 %shard_map.155 = bf16[192,4096]{1,0:T(8,128)(2,1)} custom-call(bf16[192,4096]{1,0:T(8,128)(2,1)} %shard_map.154.src), custom_call_target="tpu_custom_call" | custom-call | tf_op jit(solution)/shard_map/pallas_call | solution.py:895

commit v6 on v5

--- a/solution.py
+++ b/solution.py
@@ -272,11 +272,11 @@
                 self.paired(q, part)
 
 
-def minus_expm1(y):
-    series = 1.0 + y * (1.0 / 8.0)
-    for n in (7.0, 6.0, 5.0, 4.0, 3.0, 2.0):
+def one_minus_exp(y, grown):
+    series = 1.0 + y * (1.0 / 5.0)
+    for n in (4.0, 3.0, 2.0):
         series = 1.0 + y * (1.0 / n) * series
-    return jnp.where(y > -0.35, -y * series, 1.0 - jnp.exp(y))
+    return jnp.where(y > -0.25, -y * series, 1.0 - grown)
 
 
 def gelu(v):
@@ -519,25 +519,26 @@
 
     tile = length // 4
 
-    def project_rec(q):
-        at = pl.ds(pl.multiple_of(q * tile, tile), tile)
+    def project_rec(begin, size):
+        at = pl.ds(pl.multiple_of(begin, 64), size)
         product = jnp.dot(xall[at], rwall[...], preferred_element_type=f32).astype(bf16)
         projr[at] = product
-        rext[pl.ds(pl.multiple_of(q * tile + rtop, 16), tile)] = product[:, :rwid].astype(f32)
+        rext[pl.ds(pl.multiple_of(begin + rtop, 16), size)] = product[:, :rwid].astype(f32)
 
     @pl.loop(0, 3)
     def _(i):
-        project_rec((me.q // 2 + i // 2) % 2 * 2 + (me.q % 2 + i % 2) % 2)
+        project_rec(((me.q // 2 + i // 2) % 2 * 2 + (me.q % 2 + i % 2) % 2) * tile, tile)
 
     for n, p in enumerate(pieces):
-        cl.relay(1, p, n < 1, True)
+        cl.relay(1, p, n < 2, True)
     for i in range(xg.half):
         xg.third(i)
+    project_rec((me.qd * 2 + me.c) * rows, rows)
     xg.last(pieces[3:])
-    project_rec(me.qd)
+    project_rec((me.qd * 2 + 1 - me.c) * rows, rows)
 
     mail.send(rext.at[pl.ds(length, rtop)], rext.at[pl.ds(0, rtop)], rh.at[0], me.up, me.has_up)
-    for p in pieces[1:3]:
+    for p in pieces[2:]:
         cl.relay(1, p, True, False)
     for k in range(2, last):
         for p in pieces:
@@ -577,7 +578,7 @@
         moved = jnp.where(i % 2 == 0, wide[:, :rwid], wide[:, rwid:])
         log_decay = moved - retain * softened
         decay = jnp.exp(log_decay)
-        inflow = jnp.sqrt(minus_expm1(2.0 * log_decay)) * admit * smooth.astype(f32)
+        inflow = jnp.sqrt(one_minus_exp(log_decay, decay) * (1.0 + decay)) * admit * smooth.astype(f32)
         for f in range(fold):
             w = min(128, rwid - f * 128)
             spot = pl.ds(pl.multiple_of(i * lane_seg, 8), seg)
@@ -607,12 +608,20 @@
     for k in range(1, planes):
         mail.send(carry, cr_all.at[me.z], rc.at[me.z], lined[k - 1], me.z + k < planes)
     early = me.z < planes - 2
-    cl.relay(1, pieces[3], True, False)
     for k in range(2, last):
-        for p in pieces[:2]:
+        for p in pieces[:3]:
             cl.relay(k, p, True, False)
     for p in parts[1:]:
         out_own(p, early, True)
+
+    for i in range(SEGMENTS):
+        there = pl.ds(i * lane_seg, seg)
+        factor = gelu(projr[pl.ds(i * seg, seg), pl.ds(rwid, rwid)].astype(f32))
+        for f in range(fold):
+            w = min(128, rwid - f * 128)
+            lanes = pl.ds(0, w)
+            dec[f, there, lanes] = dec[f, there, lanes] * factor[:, f * 128 : f * 128 + w]
+            inf[f, there, lanes] = inf[f, there, lanes] * factor[:, f * 128 : f * 128 + w]
 
     for k in range(1, planes):
         z = me.z - k
@@ -631,8 +640,7 @@
     def rec_result(i):
         here, there = pl.ds(i * seg, seg), pl.ds(i * lane_seg, seg)
         state = [dec[f, there] * entering[f * SEGMENTS + i] + inf[f, there] for f in range(fold)]
-        state = jnp.concatenate(state, axis=1)[:, :rwid]
-        result = (gelu(projr[here, pl.ds(rwid, rwid)].astype(f32)) * state).astype(bf16)
+        result = jnp.concatenate(state, axis=1)[:, :rwid].astype(bf16)
         yall[here, pl.ds(pl.multiple_of(8 * cw + placed * major, 128), major)] = result[:, :major]
         return result[:, major:]
 
@@ -657,7 +665,7 @@
     for k in range(1, last):
         for p in pieces:
             cl.settle(k, p)
-        for p in pieces[2:] if k > 1 else ():
+        for p in pieces[3:] if k > 1 else ():
             cl.await_up(k, p)
     plane_depth = 4 * depth
     is_last = (me.z == last).astype(jnp.int32)
@@ -689,7 +697,7 @@
 
     finish_conv(middle)
     for k in range(2, last):
-        for p in pieces[2:]:
+        for p in pieces[3:]:
             cl.forward_up(k, p)
     for p in parts[1:]:
         out_own(p, jnp.logical_not(early), False)

time: 153 us -> 149 us (0.974)
  the two profiles are of different devices: /device:TPU:30 before, /device:TPU:0 now
where the time goes in v6:
time: 149 us
  Pallas kernels  149 us (100%)
    pallas_call x1, Pallas kernels, layer(): pl.pallas_call(functools.partial(layer_kernel, planes, lags), out_shape=j...  147 us

profile of v6, /device:TPU:0, one launch (start us, length us, event | category | flops | bytes accessed | tf_op | source)
XLA Modules:
  0.0 148.9 jit_solution(8824447607172941084)
XLA Ops:
  0.0 146.8 %shard_map.154.src = bf16[192,4096]{1,0:T(8,128)(2,1)} custom-call(bf16[192,4096]{1,0:T(8,128)(2,1)} %tokens.1, f32[1,4096]{1,0:T(1,128)} %bitcast.3, bf16[256,512]{1,0:T(8,128)(2,1)} %val_w.1, bf16[256,512]{1,0:T(8,128)(2,1)} %gate_w.1, bf16[256,768]{1,0:T(8,128)(2,1)} %rgate_w.1, bf16[256,768]{1,0:T(8,128)(2,1)} %rin_w.1, bf16[31,512]{1,0:T(8,128)(2,1)} %taps_in.1, ...), custom_call_target="tpu_custom_call" | custom-call | tf_op jit(solution)/shard_map/pallas_call | solution.py:933
  146.8 2.2 %shard_map.155 = bf16[192,4096]{1,0:T(8,128)(2,1)} custom-call(bf16[192,4096]{1,0:T(8,128)(2,1)} %shard_map.154.src), custom_call_target="tpu_custom_call" | custom-call | tf_op jit(solution)/shard_map/pallas_call | solution.py:903

commit v7 on v6

--- a/solution.py
+++ b/solution.py
@@ -173,26 +173,36 @@
 
 class Mail:
     def __init__(self, send_sem):
-        self.send_sem, self.count, self.open = send_sem, 0, []
-
-    def send(self, src, dst, recv, device, when=None):
+        self.send_sem, self.tag, self.open = send_sem, "early", []
+        self.free = list(range(send_sem.shape[0]))
+
+    def claim(self):
+        self.free.sort()
+        return self.free.pop(0)
+
+    def send(self, src, dst, recv, device, when=None, index=None):
+        index = self.claim() if index is None else index
         copy = pltpu.make_async_remote_copy(
-            src_ref=src, dst_ref=dst, send_sem=self.send_sem.at[self.count],
+            src_ref=src, dst_ref=dst, send_sem=self.send_sem.at[index],
             recv_sem=recv, device_id=device, device_id_type=MESH,
         )
-        self.count += 1
-        self.open.append((copy.wait_send, when))
+        self.open.append((self.tag, index, copy.wait_send, when))
         if when is None:
             copy.start()
         else:
             pl.when(when)(copy.start)
-
-    def local(self, src, dst):
-        copy = pltpu.make_async_copy(src, dst, self.send_sem.at[self.count])
-        self.count += 1
+        return index
+
+    def load(self, src, dst):
+        index = self.claim()
+        copy = pltpu.make_async_copy(src, dst, self.send_sem.at[index])
         copy.start()
-        self.open.append((copy.wait, None))
-        return self.open[-1]
+        return index, copy
+
+    def loaded(self, copies):
+        for index, copy in copies:
+            copy.wait()
+            self.free.append(index)
 
     def arrived(self, dst, recv, device):
         pltpu.make_async_remote_copy(
@@ -200,12 +210,15 @@
             recv_sem=recv, device_id=device, device_id_type=MESH,
         ).wait_recv()
 
-    def finish(self):
-        for wait, when in self.open:
+    def finish(self, *tags):
+        done = [entry for entry in self.open if not tags or entry[0] in tags]
+        self.open = [entry for entry in self.open if entry not in done]
+        for _, index, wait, when in done:
             if when is None:
                 wait()
             else:
                 pl.when(when)(wait)
+        self.free.extend({entry[1] for entry in done})
 
 
 def greet(me, devices, line):
@@ -292,7 +305,13 @@
         me = self.me
         for wanted, has, device in ((up, me.has_up, me.up), (down, me.has_down, me.down)):
             if wanted is not False:
-                self.mail.send(src, self.slot(me.z, piece), self.recv.at[me.z, piece], device, has & wanted)
+                self.post(src, me.z, piece, device, has & wanted)
+
+    def post(self, src, origin, piece, device, when):
+        self.mail.send(src, self.slot(origin, piece), self.recv.at[origin, piece], device, when)
+
+    def mine(self, origin):
+        return True
 
     def ways(self, k):
         me = self.me
@@ -301,19 +320,18 @@
             (me.z + k, me.z + k < self.planes, me.down, me.has_down),
         )
 
-    def take(self, origin, piece, when):
+    def take(self, origin, piece, when, index=None):
         here, sem = self.slot(origin, piece), self.recv.at[origin, piece]
         pl.when(when)(functools.partial(self.mail.arrived, here, sem, self.me.partner))
-        if self.seen is not None:
-            self.seen(origin, piece, when)
-        return here, sem
+        return None if self.seen is None else self.seen(origin, piece, when, index)
 
     def relay(self, k, piece, up=True, down=True):
         for wanted, (origin, there, on, more) in zip((up, down), self.ways(k)):
             if wanted:
                 when = jnp.logical_and(there, more)
-                here, sem = self.take(origin, piece, when)
-                self.mail.send(here, here, sem, on, when)
+                here = self.slot(origin, piece)
+                self.take(origin, piece, when)
+                self.post(here, origin, piece, on, when)
 
     def await_up(self, k, piece):
         origin, there, _, more = self.ways(k)[0]
@@ -324,9 +342,33 @@
         here, sem = self.slot(origin, piece), self.recv.at[origin, piece]
         self.mail.send(here, here, sem, on, there & more)
 
-    def settle(self, k, piece, when=True):
-        for origin, there, _, more in self.ways(k):
-            self.take(origin, piece, there & jnp.logical_not(more) & when)
+    def settle(self, k, piece):
+        me = self.me
+        lowest, highest = jnp.logical_not(me.has_down), jnp.logical_not(me.has_up)
+        origin = jnp.where(lowest, me.z + k, me.z - k)
+        here, sem = self.slot(origin, piece), self.recv.at[origin, piece]
+        pl.when((lowest | highest) & self.mine(origin))(functools.partial(self.mail.arrived, here, sem, me.partner))
+
+
+class OutLine(Line):
+    def __init__(self, me, mail, planes, slot, recv, seen, other, other_recv):
+        super().__init__(me, mail, planes, slot, recv, seen)
+        self.other, self.other_recv = other, other_recv
+
+    def mine(self, origin):
+        return origin // (self.planes // 2) == self.me.c
+
+    def post(self, src, origin, piece, device, when):
+        me = self.me
+        z = device["sp"] // 4
+        ends = (z == 0) | (z == self.planes - 1)
+        cross = ends & jnp.logical_not(self.mine(origin))
+        here, sem = self.slot(origin, piece), self.recv.at[origin, piece]
+        index = self.mail.send(src, here, sem, device, when & jnp.logical_not(cross))
+        place = origin - (1 - me.c) * (self.planes // 2)
+        sem = self.other_recv.at[place, piece]
+        device = me.at(device["sp"], 1 - me.c)
+        self.mail.send(src, self.other(place, piece), sem, device, when & cross, index)
 
 
 def small_softplus(v):
@@ -338,15 +380,16 @@
 
 
 OUT_PARTS = 4
+POOL = 84
 
 
 def layer_kernel(
     planes, lags, tokens, gain_in, val_w, gate_w, rgate_w, rin_w, taps_in, bias_in, cgain_in, staps_in,
     dmap_in, imap_in, base_in, jump_in, ocw, orw,
     out, x_ref, gain, rin_s, rgate_s, wr, wc, taps, bias, cgain, staps, dmap, imap, rbase, jump, jb, cpar, rpar,
-    ld, xall, rwall, cwall, projr, jall, wz, wp, yall, yrest, cacc, cbuf, gext, rext, filt, dec, inf, maps, ft,
+    xall, rwall, cwall, projr, jall, wz, wp, yall, yrest, cacc, cbuf, gext, rext, filt, dec, inf, maps, ft,
     st_all, carry, cr_all,
-    send, rx, rpx, rwr, rwc, zr, zc, zo, rj, ry, rp, rv, rq, re, rf, rw, rh, rs, rc, ls, lr,
+    send, rx, rpx, rwr, rwc, zrc, zo, rj, rvq, re, rf, rw, rh, rs, rc,
 ):
     me = Spot(planes)
     mail = Mail(send)
@@ -375,14 +418,8 @@
     last = planes - 1
     mates = [me.at(me.z * 4 + (me.q + dq) % 4, c) for dq in range(4) for c in (me.c, 1 - me.c)][1:]
     lined = [me.at((me.s + 4 * k) % (4 * planes), me.c) for k in range(1, planes)]
-    loads = []
-
-    def load(src, dst):
-        copy = pltpu.make_async_copy(src, dst, ld.at[len(loads)])
-        loads.append(copy)
-        copy.start()
-        return copy
-
+    crossed = [me.at((me.s + 4 * k) % (4 * planes), 1 - me.c) for k in range(1, planes)]
+    load = mail.load
     got_rec = [load(rin_w, rin_s), load(rgate_w, rgate_s)]
     got_x = [load(tokens, x_ref), load(gain_in, gain)]
     got_conv = []
@@ -404,9 +441,8 @@
             (dmap_in, dmap), (imap_in, imap), (base_in, rbase),
         )
     ]
-    greet(me, mates + lined, False)
-    for copy in got_rec:
-        copy.wait()
+    greet(me, mates + lined + crossed, False)
+    mail.loaded(got_rec)
     for q in range(4):
         lanes = slice(q * rwid, (q + 1) * rwid)
         wr[q] = jnp.concatenate([rin_s[:, lanes], rgate_s[:, lanes]], axis=1)
@@ -417,24 +453,28 @@
 
         return slot
 
-    def theirs_too(origin, piece, when):
+    def theirs_too(origin, piece, when, index=None):
         theirs = jnp.logical_and(origin // part != me.c, when)
         place = origin - (1 - me.c) * part
-        mail.send(wz.at[(origin, *cut(piece))], wp.at[(place, *cut(piece))], rw.at[place, piece], me.partner, theirs)
-
-    rl = Line(me, mail, planes, of_rows(rwall), zr)
-    cl = Line(me, mail, planes, of_rows(cwall), zc)
-    ol = Line(me, mail, planes, lambda origin, p: wz.at[(origin, *cut(p))], zo, theirs_too)
+        here, there = wz.at[(origin, *cut(piece))], wp.at[(place, *cut(piece))]
+        return mail.send(here, there, rw.at[place, piece], me.partner, theirs, index)
+
+    rl = Line(me, mail, planes, of_rows(rwall), zrc.at[0])
+    cl = Line(me, mail, planes, of_rows(cwall), zrc.at[1])
+    ol = OutLine(
+        me, mail, planes, lambda origin, p: wz.at[(origin, *cut(p))], zo, theirs_too,
+        lambda place, p: wp.at[(place, *cut(p))], rw,
+    )
 
     def out_own(p, up=True, down=True):
         ol.own(p, wz.at[(me.z, *cut(p))], up, down)
 
+    mail.tag = "first"
     for q in others:
         mail.send(wr.at[q], rl.slot(me.z, me.q), rwr.at[me.q], me.mate(q))
     rl.own(me.q, wr.at[me.q])
 
-    for copy in got_x:
-        copy.wait()
+    mail.loaded(got_x)
     first_row = mine * rows
 
     @pl.loop(0, rows // 16)
@@ -451,20 +491,15 @@
 
     xg = PlaneGather(me, mail, xslot, rx, rpx)
     xg.start()
-    for copy in got_conv + got_out:
-        copy.wait()
+    mail.loaded(got_conv + got_out)
     for q in others:
         mail.send(wc.at[q], cl.slot(me.z, me.q), rwc.at[me.q], me.mate(q))
     cl.own(me.q, wc.at[me.q])
     out_own(0)
-    kept_here = [mail.local(wr.at[me.q], rl.slot(me.z, me.q)), mail.local(wc.at[me.q], cl.slot(me.z, me.q))]
-    for entry in kept_here:
-        mail.open.remove(entry)
-        entry[0]()
+    mail.loaded([load(wr.at[me.q], rl.slot(me.z, me.q)), load(wc.at[me.q], cl.slot(me.z, me.q))])
     for p in parts:
         theirs_too(me.z, p, True)
-    for copy in got_jump + got_small:
-        copy.wait()
+    mail.loaded(got_jump + got_small)
     half = jump.shape[0] // 2
     for q in range(4):
         lanes = slice(q * rwid, (q + 1) * rwid)
@@ -500,6 +535,7 @@
         rl.own(q, here)
     for p in pieces:
         rl.relay(1, p)
+    mail.tag = "early"
     for i in range(xg.half):
         xg.first(i)
     for q in others:
@@ -529,14 +565,18 @@
     def _(i):
         project_rec(((me.q // 2 + i // 2) % 2 * 2 + (me.q % 2 + i % 2) % 2) * tile, tile)
 
+    mail.tag = "conv"
     for n, p in enumerate(pieces):
         cl.relay(1, p, n < 2, True)
+    mail.tag = "early"
     for i in range(xg.half):
         xg.third(i)
+    mail.finish("first")
     project_rec((me.qd * 2 + me.c) * rows, rows)
     xg.last(pieces[3:])
     project_rec((me.qd * 2 + 1 - me.c) * rows, rows)
 
+    mail.tag = "conv"
     mail.send(rext.at[pl.ds(length, rtop)], rext.at[pl.ds(0, rtop)], rh.at[0], me.up, me.has_up)
     for p in pieces[2:]:
         cl.relay(1, p, True, False)
@@ -611,8 +651,10 @@
     for k in range(2, last):
         for p in pieces[:3]:
             cl.relay(k, p, True, False)
+    mail.tag = "gather"
     for p in parts[1:]:
         out_own(p, early, True)
+    mail.finish("early")
 
     for i in range(SEGMENTS):
         there = pl.ds(i * lane_seg, seg)
@@ -657,11 +699,13 @@
 
         return PlaneGather(me, mail, slot, recv, recv_pair)
 
-    mg = gather(yall, 8 * cw, major, rv, rq)
+    mg = gather(yall, 8 * cw, major, rvq.at[0], rvq.at[1])
     eg = gather(yrest, 0, 2 * minor, re, rf)
-    yg = gather(yall, 0, cw, ry, rp)
+    yg = gather(yall, 0, cw, rx, rpx)
+    mail.tag = "conv"
     mg.start()
     eg.start()
+    mail.tag = "gather"
     for k in range(1, last):
         for p in pieces:
             cl.settle(k, p)
@@ -741,8 +785,11 @@
         mg.first(i)
     for i in range(eg.half):
         eg.first(i)
+    mail.tag = "out"
     for p in parts:
         ol.relay(1, p)
+    mail.tag = "gather"
+    mail.finish("conv")
 
     for k in range(1, 8):
         d = (mine + k) % 8
@@ -757,12 +804,16 @@
     gain_col = jnp.broadcast_to(cpar[pl.ds(c_lags + 2, 1), :], (8, cw)).T[:, 0:1]
     v = (ft[...] - mean) * scale * gain_col
     yall[:, pl.ds(pl.multiple_of(placed * cw, 128), cw)] = (v * jax.nn.sigmoid(v)).T.astype(bf16)
+    mail.tag = "begun"
     yg.start()
+    mail.tag = "share"
     mg.second()
     eg.second()
     for g in (mg, eg):
         for i in range(g.half):
             g.third(i)
+    mail.tag = "last"
+    mail.finish("gather")
     for i in range(yg.half):
         yg.first(i)
     for k in range(2, last):
@@ -770,6 +821,7 @@
             ol.relay(k, p)
     mg.last(pieces)
     eg.last(pieces)
+    mail.finish("share")
     rest_at = 8 * (cw + major)
 
     @pl.loop(0, SEGMENTS // 2)
@@ -789,22 +841,29 @@
 
     cols = wz.shape[2]
     upward = me.z < part
-    far = last - me.z
-    far_mine = far // part == me.c
 
     def lanes_of(h):
         return pl.ds(0, cols) if h is None else pl.ds(h * half_cols, half_cols)
 
-    def multiply(q, k, h):
+    def summed(q, k, h, low, high):
         here = pl.ds(pl.multiple_of(q * 2 * rows, 16), 2 * rows)
         total = jnp.zeros((2 * rows, cols if h is None else half_cols), f32)
         for c, block in ((me.c, wz.at[me.c * part + k]), (1 - me.c, wp.at[k])):
             begin = 0
             for at, lanes in ((0, 4 * cw), (8 * cw, 4 * major), (rest_at, 4 * minor)):
-                left = yall[here, pl.ds(pl.multiple_of(at + c * lanes, 128), lanes)]
-                right = block[pl.ds(begin, lanes), lanes_of(h)]
-                total = total + jnp.dot(left, right, preferred_element_type=f32)
+                first, end = max(begin, low), min(begin + lanes, high)
+                if first < end:
+                    spot = pl.multiple_of(at + c * lanes + first - begin, 128)
+                    right = block[pl.ds(first, end - first), lanes_of(h)]
+                    left_part = yall[here, pl.ds(spot, end - first)]
+                    total = total + jnp.dot(left_part, right, preferred_element_type=f32)
                 begin = begin + lanes
+        return here, total
+
+    def multiply(q, k, h):
+        here, total = summed(q, k, h, tall if h == 1 else 0, 2 * tall)
+        if h == 1:
+            total = total + cacc[here, pl.ds(0, half_cols)]
         total = total.astype(bf16)
         for c in range(2):
             cbuf[q * 2 + c, k, :, lanes_of(h)] = total[c * rows : (c + 1) * rows]
@@ -817,16 +876,24 @@
         flip = 3 - i
         return (me.q // 2 + flip // 2) % 2 * 2 + (me.q % 2 + flip % 2) % 2
 
+    mail.finish("begun")
+
+    def left(d, k, h):
+        return rvq.at[k, d // 2, d % 2 * 2 + (h or 0)]
+
+    def landed(d, k, h):
+        return zrc.at[k, d // 2, d % 2 * 2 + (h or 0)]
+
     def parcel(q, c, k, h):
         return pltpu.make_async_remote_copy(
             src_ref=cbuf.at[q * 2 + c, k, :, lanes_of(h)], dst_ref=place(me.q, me.c, k, h),
-            send_sem=ls.at[q * 2 + c, k, h or 0], recv_sem=lr.at[mine, k, h or 0],
+            send_sem=left(q * 2 + c, k, h), recv_sem=landed(mine, k, h),
             device_id=me.at(me.z * 4 + q, c), device_id_type=MESH,
         )
 
     def kept(k, h):
         src = cbuf.at[mine, k, :, lanes_of(h)]
-        return pltpu.make_async_copy(src, place(me.q, me.c, k, h), ls.at[mine, k, h or 0])
+        return pltpu.make_async_copy(src, place(me.q, me.c, k, h), left(mine, k, h))
 
     def serve(q, k, h):
         multiply(q, k, h)
@@ -854,28 +921,36 @@
     for n in range(1, part - 1):
         ready(order[n], parts)
         pl.loop(0, 4)(lambda i: serve(mate_of(i), order[n], None))
-    for h in range(2):
-        halves = parts[2 * h : 2 * h + 2]
-        for p in halves:
-            ol.settle(last, p, far_mine)
-        ready(order[-1], halves)
-        pl.loop(0, 4)(lambda i: serve(mate_of(i), order[-1], h))
-    for p in parts:
-        ol.settle(last, p, jnp.logical_not(far_mine))
+    k_far = order[-1]
+    for p in parts[:2]:
+        ol.settle(last, p)
+    ready(k_far, parts[:2])
+    pl.loop(0, 4)(lambda i: serve(mate_of(i), k_far, 0))
+    ol.settle(last, 2)
+    ready(k_far, parts[2:3])
+
+    @pl.loop(0, 4)
+    def _(q):
+        here, total = summed(q, k_far, 1, 0, tall)
+        cacc[here, pl.ds(0, half_cols)] = total
+
+    ol.settle(last, 3)
+    ready(k_far, parts[3:])
+    pl.loop(0, 4)(lambda i: serve(mate_of(i), k_far, 1))
     rounds = [(k, None) for k in order[:-1]] + [(order[-1], 0), (order[-1], 1)]
 
     @pl.loop(0, 4)
     def _(i):
         q = mate_of(i)
         for k, h in rounds:
-            mail.arrived(place(q, 1 - me.c, k, h), lr.at[q * 2 + 1 - me.c, k, h or 0], me.partner)
+            mail.arrived(place(q, 1 - me.c, k, h), landed(q * 2 + 1 - me.c, k, h), me.partner)
             parcel(q, 1 - me.c, k, h).wait_send()
 
     @pl.loop(0, 3)
     def _(i):
         q = mate_of(i)
         for k, h in rounds:
-            mail.arrived(place(q, me.c, k, h), lr.at[q * 2 + me.c, k, h or 0], me.partner)
+            mail.arrived(place(q, me.c, k, h), landed(q * 2 + me.c, k, h), me.partner)
             parcel(q, me.c, k, h).wait_send()
 
     for k, h in rounds:
@@ -941,7 +1016,6 @@
             vmem(*taps.shape), wide(1, 4 * cw), wide(1, 4 * cw), vmem(*staps.shape),
             vmem(*dmap.shape), vmem(*imap.shape), wide(4 * rwid), wide(*jump.shape),
             vmem(4, jump.shape[0] // 2, 2 * rwid), wide(lags[0] + 3 + -(lags[0] + 3) % 8, cw), wide(8, rwid),
-            dma((32,)),
             vmem(length, width_in),
             vmem(deep, 2 * rwid),
             vmem(deep, 2 * cw),
@@ -963,10 +1037,10 @@
             wide(8, 2, length),
             wide(8, 128),
             wide(planes, 8, 128),
-            dma((180 + 20 * planes,)), dma((4, 4)), dma((4, 4)), dma((4,)), dma((4,)),
-            dma((planes, 4)), dma((planes, 4)), dma((planes, OUT_PARTS)), dma((4,)),
-            dma((4, 4)), dma((4, 4)), dma((4, 4)), dma((4, 4)), dma((4, 2)), dma((4, 2)), dma((part, OUT_PARTS)),
-            dma((2,)), dma((8,)), dma((planes,)), dma((8, part, 2)), dma((8, part, 2)),
+            dma((POOL,)), dma((4, 4)), dma((4, 4)), dma((4,)), dma((4,)),
+            dma((part, planes, 4)), dma((planes, OUT_PARTS)), dma((4,)),
+            dma((part, 4, 4)), dma((4, 2)), dma((4, 2)), dma((part, OUT_PARTS)),
+            dma((2,)), dma((8,)), dma((planes,)),
         ],
         compiler_params=pltpu.CompilerParams(
             collective_id=0, has_side_effects=True, vmem_limit_bytes=60 * 1024 * 1024

time: 149 us -> 145 us (0.973)
  Pallas kernels: 149 us -> 144 us
    pallas_call x1, Pallas kernels: 147 us -> 142 us  [layer(): pl.pallas_call(functools.partial(layer_kernel, planes, lags), out_shape=j...]
where the time goes in v7:
time: 145 us; the launch traced here: 144 us
  Pallas kernels  144 us (99%)
    pallas_call x1, Pallas kernels, layer(): pl.pallas_call(functools.partial(layer_kernel, planes, lags), out_shape=j...  142 us

profile of v7, /device:TPU:0, one launch (start us, length us, event | category | flops | bytes accessed | tf_op | source)
XLA Modules:
  0.0 143.8 jit_solution(11631521732850800084)
XLA Ops:
  0.0 141.6 %shard_map.154.src = bf16[192,4096]{1,0:T(8,128)(2,1)} custom-call(bf16[192,4096]{1,0:T(8,128)(2,1)} %tokens.1, f32[1,4096]{1,0:T(1,128)} %bitcast.3, bf16[256,512]{1,0:T(8,128)(2,1)} %val_w.1, bf16[256,512]{1,0:T(8,128)(2,1)} %gate_w.1, bf16[256,768]{1,0:T(8,128)(2,1)} %rgate_w.1, bf16[256,768]{1,0:T(8,128)(2,1)} %rin_w.1, bf16[31,512]{1,0:T(8,128)(2,1)} %taps_in.1, ...), custom_call_target="tpu_custom_call" | custom-call | tf_op jit(solution)/shard_map/pallas_call | solution.py:1008
  141.6 2.2 %shard_map.155 = bf16[192,4096]{1,0:T(8,128)(2,1)} custom-call(bf16[192,4096]{1,0:T(8,128)(2,1)} %shard_map.154.src), custom_call_target="tpu_custom_call" | custom-call | tf_op jit(solution)/shard_map/pallas_call | solution.py:978

commit v8 on v7

--- a/solution.py
+++ b/solution.py
@@ -283,6 +283,36 @@
         for q in origins:
             for part in range(self.parts):
                 self.paired(q, part)
+
+
+class RowGather(PlaneGather):
+    def start(self):
+        me, mail = self.me, self.mail
+        for to_x, to_y in ((me.qx, me.qy), (me.q, me.qd), (me.qd, me.q), (me.qy, me.qx)):
+            for q, part in ((me.qx, to_x), (me.qy, to_y)):
+                own = self.slot(me.q, me.c, part)
+                mail.send(own, own, self.recv.at[me.q, part], me.mate(q))
+        for part in range(self.parts):
+            self.share(me.q, part, self.slot(me.q, me.c, part))
+
+    def first(self, i):
+        me = self.me
+        part = (me.q, me.qx)[i]
+        for q, to in ((me.qx, me.qy), (me.qy, me.qx)):
+            here = self.took(q, part)
+            self.mail.send(here, here, self.recv.at[q, part], me.mate(to))
+            self.share(q, part, here)
+
+    def second(self):
+        me = self.me
+        for part in (me.qd, me.qy):
+            for q in (me.qx, me.qy):
+                self.share(q, part, self.took(q, part))
+
+    def third(self, i):
+        me = self.me
+        for part in ((me.qx, me.qy), (me.q, me.qd))[i]:
+            self.share(me.qd, part, self.took(me.qd, part))
 
 
 def one_minus_exp(y, grown):
@@ -571,28 +601,9 @@
     mail.tag = "early"
     for i in range(xg.half):
         xg.third(i)
-    mail.finish("first")
-    project_rec((me.qd * 2 + me.c) * rows, rows)
-    xg.last(pieces[3:])
-    project_rec((me.qd * 2 + 1 - me.c) * rows, rows)
-
-    mail.tag = "conv"
-    mail.send(rext.at[pl.ds(length, rtop)], rext.at[pl.ds(0, rtop)], rh.at[0], me.up, me.has_up)
-    for p in pieces[2:]:
-        cl.relay(1, p, True, False)
-    for k in range(2, last):
-        for p in pieces:
-            cl.relay(k, p, False, True)
-
-    @pl.when(jnp.logical_not(me.has_down))
-    def _():
-        rext[pl.ds(0, rtop)] = jnp.zeros((rtop, rwid), f32)
-        gext[pl.ds(0, top)] = jnp.zeros((top, cw), f32)
-
     softened = rpar[pl.ds(s_lags + 1, 1), :]
 
-    @pl.loop(0, SEGMENTS)
-    def _(n):
+    def gate_segment(n):
         step = (n + 1) // 2
         ring = (me.q // 2 + step % 4 // 2) % 2 * 2 + (me.q % 2 + step % 2) % 2
         i = jnp.where(n == SEGMENTS - 1, 2 * me.q, 2 * ring + n % 2)
@@ -624,6 +635,27 @@
             spot = pl.ds(pl.multiple_of(i * lane_seg, 8), seg)
             dec[f, spot, pl.ds(0, w)] = decay[:, f * 128 : f * 128 + w]
             inf[f, spot, pl.ds(0, w)] = inflow[:, f * 128 : f * 128 + w]
+
+    mail.finish("first")
+    project_rec((me.qd * 2 + me.c) * rows, rows)
+    pl.loop(0, 1)(gate_segment)
+    xg.last(pieces[3:])
+    project_rec((me.qd * 2 + 1 - me.c) * rows, rows)
+
+    mail.tag = "conv"
+    mail.send(rext.at[pl.ds(length, rtop)], rext.at[pl.ds(0, rtop)], rh.at[0], me.up, me.has_up)
+    for p in pieces[2:]:
+        cl.relay(1, p, True, False)
+    for k in range(2, last):
+        for p in pieces:
+            cl.relay(k, p, False, True)
+
+    @pl.when(jnp.logical_not(me.has_down))
+    def _():
+        rext[pl.ds(0, rtop)] = jnp.zeros((rtop, rwid), f32)
+        gext[pl.ds(0, top)] = jnp.zeros((top, cw), f32)
+
+    pl.loop(1, SEGMENTS)(gate_segment)
 
     def one(i, held):
         after = []
@@ -690,18 +722,18 @@
         pair = jnp.concatenate([rec_result(i), rec_result(i + SEGMENTS // 2)], axis=1)
         yrest[pl.ds(i * seg, seg), pl.ds(pl.multiple_of(placed * 2 * minor, 128), 2 * minor)] = pair
 
-    def gather(buffer, lane, lanes, recv, recv_pair):
+    def gather(buffer, lane, lanes, recv, recv_pair, kind=PlaneGather):
         tall_part = buffer.shape[0] // recv.shape[1]
 
         def slot(q, c, h):
             spot = pl.ds(pl.multiple_of(lane + (c * 4 + q) * lanes, 128), lanes)
-            return buffer.at[pl.ds(h * tall_part, tall_part), spot]
-
-        return PlaneGather(me, mail, slot, recv, recv_pair)
+            return buffer.at[pl.ds(pl.multiple_of(h * tall_part, 16), tall_part), spot]
+
+        return kind(me, mail, slot, recv, recv_pair)
 
     mg = gather(yall, 8 * cw, major, rvq.at[0], rvq.at[1])
     eg = gather(yrest, 0, 2 * minor, re, rf)
-    yg = gather(yall, 0, cw, rx, rpx)
+    yg = gather(yall, 0, cw, rx, rpx, RowGather)
     mail.tag = "conv"
     mg.start()
     eg.start()
@@ -911,12 +943,12 @@
         if i:
             yg.third(i)
         for q in pieces:
-            yg.paired(q, i)
-            yg.paired(q, yg.half + i)
+            for row_part in ((me.qx, me.qy), (me.q, me.qd))[i]:
+                yg.paired(q, row_part)
 
         @pl.loop(0, 2)
         def _(n):
-            serve(n * yg.half + i, order[0], None)
+            serve(mate_of(3 - 3 * (1 - n) if i else 2 - n), order[0], None)
 
     for n in range(1, part - 1):
         ready(order[n], parts)

time: 145 us -> 144 us (level)
  no operation moved by 1% of the time
where the time goes in v8:
time: 144 us
  Pallas kernels  144 us (100%)
    pallas_call x1, Pallas kernels, layer(): pl.pallas_call(functools.partial(layer_kernel, planes, lags), out_shape=j...  142 us

profile of v8, /device:TPU:0, one launch (start us, length us, event | category | flops | bytes accessed | tf_op | source)
XLA Modules:
  0.0 143.7 jit_solution(17533987915995657079)
XLA Ops:
  0.0 141.5 %shard_map.154.src = bf16[192,4096]{1,0:T(8,128)(2,1)} custom-call(bf16[192,4096]{1,0:T(8,128)(2,1)} %tokens.1, f32[1,4096]{1,0:T(1,128)} %bitcast.3, bf16[256,512]{1,0:T(8,128)(2,1)} %val_w.1, bf16[256,512]{1,0:T(8,128)(2,1)} %gate_w.1, bf16[256,768]{1,0:T(8,128)(2,1)} %rgate_w.1, bf16[256,768]{1,0:T(8,128)(2,1)} %rin_w.1, bf16[31,512]{1,0:T(8,128)(2,1)} %taps_in.1, ...), custom_call_target="tpu_custom_call" | custom-call | tf_op jit(solution)/shard_map/pallas_call | solution.py:1040
  141.5 2.2 %shard_map.155 = bf16[192,4096]{1,0:T(8,128)(2,1)} custom-call(bf16[192,4096]{1,0:T(8,128)(2,1)} %shard_map.154.src), custom_call_target="tpu_custom_call" | custom-call | tf_op jit(solution)/shard_map/pallas_call | solution.py:1010

commit v9 on v8

--- a/solution.py
+++ b/solution.py
@@ -226,12 +226,12 @@
     for device in devices:
         pl.semaphore_signal(barrier, inc=1, device_id=device, device_id_type=MESH)
     amount = len(devices)
-    if line:
-        for has, device in ((me.has_up, me.up), (me.has_down, me.down)):
-            @pl.when(has)
-            def _():
+    for has, neighbours in line:
+        @pl.when(has)
+        def _():
+            for device in neighbours:
                 pl.semaphore_signal(barrier, inc=1, device_id=device, device_id_type=MESH)
-        amount = amount + me.has_up.astype(jnp.int32) + me.has_down.astype(jnp.int32)
+        amount = amount + len(neighbours) * has.astype(jnp.int32)
     pl.semaphore_wait(barrier, amount)
 
 
@@ -448,7 +448,6 @@
     last = planes - 1
     mates = [me.at(me.z * 4 + (me.q + dq) % 4, c) for dq in range(4) for c in (me.c, 1 - me.c)][1:]
     lined = [me.at((me.s + 4 * k) % (4 * planes), me.c) for k in range(1, planes)]
-    crossed = [me.at((me.s + 4 * k) % (4 * planes), 1 - me.c) for k in range(1, planes)]
     load = mail.load
     got_rec = [load(rin_w, rin_s), load(rgate_w, rgate_s)]
     got_x = [load(tokens, x_ref), load(gain_in, gain)]
@@ -471,7 +470,8 @@
             (dmap_in, dmap), (imap_in, imap), (base_in, rbase),
         )
     ]
-    greet(me, mates + lined + crossed, False)
+    above, below = (me.up, me.at(me.s + 4, 1 - me.c)), (me.down, me.at(me.s - 4, 1 - me.c))
+    greet(me, mates, ((me.has_up, above), (me.has_down, below)))
     mail.loaded(got_rec)
     for q in range(4):
         lanes = slice(q * rwid, (q + 1) * rwid)

time: 144 us -> 143 us (level)
  no operation moved by 1% of the time
where the time goes in v9:
time: 143 us
  Pallas kernels  143 us (100%)
    pallas_call x1, Pallas kernels, layer(): pl.pallas_call(functools.partial(layer_kernel, planes, lags), out_shape=j...  140 us

profile of v9, /device:TPU:0, one launch (start us, length us, event | category | flops | bytes accessed | tf_op | source)
XLA Modules:
  0.0 142.7 jit_solution(8939936602370740784)
XLA Ops:
  0.0 140.5 %shard_map.154.src = bf16[192,4096]{1,0:T(8,128)(2,1)} custom-call(bf16[192,4096]{1,0:T(8,128)(2,1)} %tokens.1, f32[1,4096]{1,0:T(1,128)} %bitcast.3, bf16[256,512]{1,0:T(8,128)(2,1)} %val_w.1, bf16[256,512]{1,0:T(8,128)(2,1)} %gate_w.1, bf16[256,768]{1,0:T(8,128)(2,1)} %rgate_w.1, bf16[256,768]{1,0:T(8,128)(2,1)} %rin_w.1, bf16[31,512]{1,0:T(8,128)(2,1)} %taps_in.1, ...), custom_call_target="tpu_custom_call" | custom-call | tf_op jit(solution)/shard_map/pallas_call | solution.py:1040
  140.5 2.2 %shard_map.155 = bf16[192,4096]{1,0:T(8,128)(2,1)} custom-call(bf16[192,4096]{1,0:T(8,128)(2,1)} %shard_map.154.src), custom_call_target="tpu_custom_call" | custom-call | tf_op jit(solution)/shard_map/pallas_call | solution.py:1010

commit v10 on v9

--- a/solution.py
+++ b/solution.py
@@ -786,10 +786,6 @@
     def filter_strip(n):
         i = strips - 1 - n
 
-        @pl.when(jnp.logical_and(i == 0, me.has_down))
-        def _():
-            mail.arrived(gext.at[pl.ds(0, top)], rh.at[1], me.partner)
-
         base = pl.multiple_of(i * 64, 8)
         window = gext[pl.ds(base, 64 + top)]
         total = jnp.zeros((64, cw), f32) + cpar[pl.ds(c_lags + 1, 1), :]
@@ -803,7 +799,11 @@
             total = total + shifted[r : r + 64]
         filt[pl.ds(base, 64)] = total
 
-    pl.loop(0, strips)(filter_strip)
+    pl.loop(0, strips - 2, unroll=2)(filter_strip)
+    filter_strip(strips - 2)
+    tail_halo = gext.at[pl.ds(0, top)]
+    pl.when(me.has_down)(functools.partial(mail.arrived, tail_halo, rh.at[1], me.partner))
+    filter_strip(strips - 1)
 
     turned = filt[...].T
     ft[...] = turned

time: 143 us -> 143 us (level)
  no operation moved by 1% of the time
where the time goes in v10:
time: 143 us
  Pallas kernels  143 us (100%)
    pallas_call x1, Pallas kernels, layer(): pl.pallas_call(functools.partial(layer_kernel, planes, lags), out_shape=j...  140 us

profile of v10, /device:TPU:0, one launch (start us, length us, event | category | flops | bytes accessed | tf_op | source)
XLA Modules:
  0.0 142.8 jit_solution(10015744513848091476)
XLA Ops:
  0.0 140.5 %shard_map.154.src = bf16[192,4096]{1,0:T(8,128)(2,1)} custom-call(bf16[192,4096]{1,0:T(8,128)(2,1)} %tokens.1, f32[1,4096]{1,0:T(1,128)} %bitcast.3, bf16[256,512]{1,0:T(8,128)(2,1)} %val_w.1, bf16[256,512]{1,0:T(8,128)(2,1)} %gate_w.1, bf16[256,768]{1,0:T(8,128)(2,1)} %rgate_w.1, bf16[256,768]{1,0:T(8,128)(2,1)} %rin_w.1, bf16[31,512]{1,0:T(8,128)(2,1)} %taps_in.1, ...), custom_call_target="tpu_custom_call" | custom-call | tf_op jit(solution)/shard_map/pallas_call | solution.py:1040
  140.5 2.2 %shard_map.155 = bf16[192,4096]{1,0:T(8,128)(2,1)} custom-call(bf16[192,4096]{1,0:T(8,128)(2,1)} %shard_map.154.src), custom_call_target="tpu_custom_call" | custom-call | tf_op jit(solution)/shard_map/pallas_call | solution.py:1010
